TPU v7x, 32 devices: a whole 2x2x4 slice. The times are simulated.
32 devices in a mesh: sp: 4 (over z), fs: 4 (over y, x), tp: 2 (over core).
Axes of the slice: x: 2, y: 2, z: 4, core: 2. Of those that a mesh axis runs over, the one named last changes fastest.
Arguments:
- tokens: bfloat16 [4, 3072, 2048], P('fs', 'sp'), may hold values from -6 to 6
- norm_gain: float32 [2048], replicated, may hold values from 0.1 to 1.9
- query_weight: bfloat16 [2048, 512], P(('sp', 'fs'), 'tp'), may hold values from -0.125 to 0.125
- key_weight: bfloat16 [2048, 512], P(('sp', 'fs'), 'tp'), may hold values from -0.125 to 0.125
- value_weight: bfloat16 [2048, 1024], P(('sp', 'fs'), 'tp'), may hold values from -0.125 to 0.125
- gate_weight: bfloat16 [2048, 1024], P(('sp', 'fs'), 'tp'), may hold values from -0.125 to 0.125
- conv_b_weight: bfloat16 [2048, 1024], P(('sp', 'fs'), 'tp'), may hold values from -0.125 to 0.125
- conv_c_weight: bfloat16 [2048, 1024], P(('sp', 'fs'), 'tp'), may hold values from -0.125 to 0.125
- conv_in_weight: bfloat16 [2048, 1024], P(('sp', 'fs'), 'tp'), may hold values from -0.125 to 0.125
- conv_kernel: float32 [3, 1024], P(None, 'tp'), may hold values from -3.5 to 3.5
- out_ret_weight: bfloat16 [2048, 1024], P(('sp', 'fs'), 'tp'), may hold values from -0.125 to 0.125
- out_conv_weight: bfloat16 [2048, 1024], P(('sp', 'fs'), 'tp'), may hold values from -0.125 to 0.125
- log_decay: float32 [4, 8, 3072], P('fs', 'tp', 'sp'), may hold values from -3 to 0, as said below
Outputs:
- mixed: bfloat16 [4, 3072, 2048], P('fs', ('sp', 'tp'))
Inputs may be any that keep to these rules, and one draw needn't show every extreme that they name: log_decay is never positive.
All inputs are finite; a program needn't handle non-finite values.
Results may differ from a plain program's by a relative error of at most 0.02.
Values may be sent and summed in bfloat16 or wider, within the bound.
A program may use at most 64 MiB of HBM per device.

v0:
```python
import jax
import jax.numpy as jnp
from jax import lax
from jax.experimental import pallas as pl
from jax.experimental.pallas import tpu as pltpu
from jax.sharding import PartitionSpec as P

KEY_DIM = 64
VALUE_DIM = 128
CONV_TAPS = 3
BLOCK_LEN = 128


EPSILON = 1e-06
ROPE_BASE = 10000.0


def entering(x, axis, combine, identity):
    length, here = (lax.axis_size(axis), lax.axis_index(axis))
    everything = jax.tree.map(
        lambda part, kind: lax.all_gather(part.astype(kind), axis), x, (jnp.bfloat16, jnp.bfloat16)
    )
    start = jax.tree.map(
        lambda part, zero: jnp.broadcast_to(jnp.asarray(zero, part.dtype), part.shape), x, identity
    )

    def lap(k, before):
        reached = k < here
        new = combine(
            before, jax.tree.map(lambda part, own: part[k].astype(own.dtype), everything, x)
        )
        return jax.tree.map(lambda a, b: jnp.where(reached, a, b), new, before)

    return lax.fori_loop(0, length, lap, start)


def passed_along(value, axis, steps):
    count = lax.axis_size(axis)
    first, last = (max(0, -steps), min(count, count - steps))
    return lax.ppermute(value, axis, [(source, source + steps) for source in range(first, last)])


def rotate(values, token_ordinal):
    half_dim = values.shape[-1] // 2
    frequency = 1.0 / ROPE_BASE ** jnp.linspace(0.0, 1.0, half_dim, dtype=jnp.float32)
    angles = token_ordinal[:, None] * frequency[None, :]
    cosine_table = jnp.cos(angles)[:, None, :]
    sine_table = jnp.sin(angles)[:, None, :]
    first = values[..., :half_dim].astype(jnp.float32)
    second = values[..., half_dim:].astype(jnp.float32)
    return jnp.concatenate(
        [first * cosine_table - second * sine_table, first * sine_table + second * cosine_table],
        axis=-1,
    )


def make_adder(normed, contracted, pieces):
    updated = []
    for member in range(len(pieces)):
        portion = pieces[member]
        if member < contracted:
            updated.append(jnp.dot(normed, portion, preferred_element_type=jnp.float32))
        else:
            updated.append(portion)
    return tuple(updated)


def retention_local(projections, decays, token_ordinal):
    tok_rows = token_ordinal.shape[0]
    head_count = decays.shape[0]
    blocks = tok_rows // BLOCK_LEN
    query_raw = projections[0].reshape(tok_rows, head_count, KEY_DIM)
    key_raw = projections[1].reshape(tok_rows, head_count, KEY_DIM)
    queries = rotate(query_raw, token_ordinal).astype(jnp.bfloat16)
    lookup_matrix_lines = (rotate(key_raw, token_ordinal) * KEY_DIM ** (-0.5)).astype(jnp.bfloat16)
    value_proj = projections[2].reshape(tok_rows, head_count, VALUE_DIM)

    def split_blocks(array):
        shaped = array.reshape(blocks, BLOCK_LEN, head_count, array.shape[-1])
        return jnp.transpose(shaped, (0, 2, 1, 3))

    query_blocks = split_blocks(queries)
    key_blocks = split_blocks(lookup_matrix_lines)
    value_blocks = split_blocks(value_proj)
    decay_blocks = jnp.transpose(decays.reshape(head_count, blocks, BLOCK_LEN), (1, 0, 2))
    cumulative = jnp.cumsum(decay_blocks, axis=-1)
    ending = cumulative[..., -1:]
    decay_gaps = cumulative[..., :, None] - cumulative[..., None, :]
    causal = jnp.arange(BLOCK_LEN)[:, None] >= jnp.arange(BLOCK_LEN)[None, :]
    weighting = jnp.where(causal, jnp.exp(jnp.minimum(decay_gaps, 0.0)), 0.0)
    raw_scores = jnp.einsum(
        "nhid,nhjd->nhij", query_blocks, key_blocks, preferred_element_type=jnp.float32
    )
    scores = (raw_scores * weighting).astype(jnp.bfloat16)
    intra_out = jnp.einsum(
        "nhij,nhje->nhie", scores, value_blocks, preferred_element_type=jnp.float32
    )
    decayed_keys = (
        key_blocks.astype(jnp.float32) * jnp.exp(ending - cumulative)[..., None]
    ).astype(jnp.bfloat16)
    decayed_queries = (query_blocks.astype(jnp.float32) * jnp.exp(cumulative)[..., None]).astype(
        jnp.bfloat16
    )
    block_kv = jnp.einsum(
        "nhjd,nhje->nhde", decayed_keys, value_blocks, preferred_element_type=jnp.float32
    )
    block_ends = ending[..., 0]

    def advance(state_now, step_in):
        kv_block, total = step_in
        return (state_now * jnp.exp(total)[:, None, None] + kv_block, state_now)

    start_state = jnp.zeros((head_count, KEY_DIM, VALUE_DIM), jnp.float32)
    end_state, before_local = lax.scan(advance, start_state, (block_kv, block_ends))
    device_total = jnp.sum(block_ends, axis=0)
    return (intra_out, decayed_queries, before_local, block_ends, end_state, device_total)


def combine(earlier, later):
    return (earlier[0] * jnp.exp(later[1])[:, None, None] + later[0], earlier[1] + later[1])


def carried(end_state, device_total):
    identity = (jnp.zeros_like(end_state), jnp.zeros_like(device_total))
    state_in, _ = entering((end_state, device_total), "sp", combine, identity)
    return state_in


def retention_finish(local_parts, state_in, gate_proj):
    intra_out, decayed_queries, before_local, block_ends, end_state, device_total = local_parts
    starts = jnp.cumsum(block_ends, axis=0) - block_ends
    full_states = before_local + jnp.exp(starts)[:, :, None, None] * state_in[None]
    cross = jnp.einsum(
        "nhid,nhde->nhie",
        decayed_queries,
        full_states.astype(jnp.bfloat16),
        preferred_element_type=jnp.float32,
    )
    output = intra_out + cross
    output = output * lax.rsqrt(jnp.mean(output * output, axis=-1, keepdims=True) + EPSILON)
    tok_rows = gate_proj.shape[0]
    output = jnp.transpose(output, (0, 2, 1, 3)).reshape(tok_rows, gate_proj.shape[1])
    return (output * jax.nn.silu(gate_proj.astype(jnp.float32))).astype(jnp.bfloat16)


def convolve(conv_proj, conv_kernel):
    gate_b, gate_c, conv_input = conv_proj
    tok_rows = gate_b.shape[0]
    product = gate_c.astype(jnp.float32) * conv_input.astype(jnp.float32)
    rim_rows = passed_along(product[tok_rows - (CONV_TAPS - 1) :], "sp", 1)
    padded = jnp.concatenate([rim_rows, product], axis=0)
    convolved = jnp.zeros_like(product)
    for tap_index in range(CONV_TAPS):
        convolved = convolved + conv_kernel[tap_index] * padded[tap_index : tap_index + tok_rows]
    return (gate_b.astype(jnp.float32) * convolved).astype(jnp.bfloat16)


def shards(
    tokens,
    norm_gain,
    query_weight,
    key_weight,
    value_weight,
    gate_weight,
    conv_b_weight,
    conv_c_weight,
    conv_in_weight,
    conv_kernel,
    out_ret_weight,
    out_conv_weight,
    log_decay,
):
    inputs = tokens[0].astype(jnp.float32)
    tok_rows = inputs.shape[0]
    normed = (
        inputs * lax.rsqrt(jnp.mean(inputs * inputs, axis=-1, keepdims=True) + EPSILON) * norm_gain
    ).astype(jnp.bfloat16)
    token_ordinal = (
        lax.axis_index("sp") * tok_rows + jnp.arange(tok_rows, dtype=jnp.int32)
    ).astype(jnp.float32)
    decays = log_decay[0]
    gathered = make_adder(
        normed,
        7,
        (
            lax.all_gather(query_weight, ("sp", "fs"), axis=0, tiled=True),
            lax.all_gather(key_weight, ("sp", "fs"), axis=0, tiled=True),
            lax.all_gather(value_weight, ("sp", "fs"), axis=0, tiled=True),
            lax.all_gather(gate_weight, ("sp", "fs"), axis=0, tiled=True),
            lax.all_gather(conv_b_weight, ("sp", "fs"), axis=0, tiled=True),
            lax.all_gather(conv_c_weight, ("sp", "fs"), axis=0, tiled=True),
            lax.all_gather(conv_in_weight, ("sp", "fs"), axis=0, tiled=True),
            lax.all_gather(out_ret_weight, ("sp", "fs"), axis=0, tiled=True),
            lax.all_gather(out_conv_weight, ("sp", "fs"), axis=0, tiled=True),
        ),
    )
    ret_proj = [member.astype(jnp.bfloat16) for member in gathered[:4]]
    local_parts = retention_local(ret_proj, decays, token_ordinal)
    state_in = carried(local_parts[4], local_parts[5])
    conv_proj = [member.astype(jnp.bfloat16) for member in gathered[4:7]]
    full_ret, full_conv = (gathered[7], gathered[8])
    conv_out = convolve(conv_proj, conv_kernel)
    ret_out = retention_finish(local_parts, state_in, ret_proj[3])
    partial_value = lax.dot_general(
        ret_out, full_ret, (((1,), (1,)), ((), ())), preferred_element_type=jnp.float32
    )
    mixed = lax.psum_scatter(
        (
            partial_value
            + lax.dot_general(
                conv_out, full_conv, (((1,), (1,)), ((), ())), preferred_element_type=jnp.float32
            )
        ).astype(jnp.bfloat16),
        "tp",
        scatter_dimension=0,
        tiled=True,
    )
    return mixed[None]


MESH_IDS = pl.DeviceIdType.MESH


def remote(source, target, sent, landed, device):
    return pltpu.make_async_remote_copy(
        src_ref=source,
        dst_ref=target,
        send_sem=sent,
        recv_sem=landed,
        device_id=device,
        device_id_type=MESH_IDS,
    )


def greet(peers):
    barrier = pltpu.get_barrier_semaphore()
    for peer in peers:
        pl.semaphore_signal(barrier, inc=1, device_id=peer, device_id_type=MESH_IDS)
    pl.semaphore_wait(barrier, len(peers))


def plane_partners(f):
    x, y = f % 2, f // 2
    return y * 2 + (1 - x), (1 - y) * 2 + x, 3 - f


def gather_kernel(
    n_sp,
    half_ref,
    weight_ref,
    decay_ref,
    out_ref,
    proj_ref,
    decays_ref,
    outs_ref,
    normed_ref,
    full_ref,
    norm_sent,
    norm_landed,
    side_sent,
    side_landed,
    relay_sent,
    weight_sent,
    weight_landed,
    up_sent,
    down_sent,
    line_landed,
    decay_sent,
    decay_landed,
    local_sem,
    out_up_sent,
    out_down_sent,
    out_line_landed,
    out_plane_sent,
    out_plane_landed,
    out_relay_sent,
):
    s, f, t = lax.axis_index("sp"), lax.axis_index("fs"), lax.axis_index("tp")
    xn, yn, dn = plane_partners(f)
    half = half_ref.shape[0]
    chunk = half // 2
    rows = weight_ref.shape[1]
    n_fs = weight_ref.shape[0]
    other = {"tp": 1 - t}
    peers = [{"fs": xn}, {"fs": yn}, {"fs": dn}, other]
    peers += [{"sp": (s + d) % n_sp} for d in range(1, n_sp)]
    greet(peers)

    def spot(owner, core, piece):
        return normed_ref.at[owner, pl.ds(core * half + piece * chunk, chunk), :]

    def own(piece):
        return half_ref.at[pl.ds(piece * chunk, chunk), :]

    def outs(b, g):
        return outs_ref.at[pl.ds((b * n_fs + g) * rows, rows), :]

    def block(b, g):
        return full_ref.at[pl.ds((b * n_fs + g) * rows, rows), :]

    waits = []
    locals_ = []

    def start(copy):
        copy.start()
        waits.append(copy)

    order = (xn, yn, dn)
    for i, p in enumerate(order):
        start(remote(weight_ref.at[p], block(s, f), weight_sent.at[i], weight_landed.at[f], {"fs": p}))
    for i, p in enumerate(order):
        start(remote(decay_ref.at[p], decays_ref.at[f], decay_sent.at[i], decay_landed.at[f], {"fs": p}))
    start(remote(own(0), spot(f, t, 0), norm_sent.at[0], norm_landed.at[f, 0], {"fs": xn}))
    start(remote(own(1), spot(f, t, 1), norm_sent.at[1], norm_landed.at[f, 1], {"fs": yn}))
    start(remote(own(1), spot(f, t, 1), norm_sent.at[2], norm_landed.at[f, 1], {"fs": xn}))
    start(remote(own(0), spot(f, t, 0), norm_sent.at[3], norm_landed.at[f, 0], {"fs": yn}))

    def line_copy(source, b, g, way):
        sent = up_sent if way == 1 else down_sent
        return remote(source, block(b, g), sent.at[b, g], line_landed.at[b, g], {"sp": s + way})

    def send_line(source, b, g):
        @pl.when(s < n_sp - 1)
        def _():
            line_copy(source, b, g, 1).start()

        @pl.when(s > 0)
        def _():
            line_copy(source, b, g, -1).start()

    def out_line(source, b, way):
        sent = out_up_sent if way == 1 else out_down_sent
        return remote(source, outs(b, f), sent.at[b], out_line_landed.at[b], {"sp": s + way})

    def out_plane(source, b, i):
        return remote(
            source, outs(b, f), out_plane_sent.at[b, i], out_plane_landed.at[b, f], {"fs": order[i]}
        )

    send_line(weight_ref.at[f], s, f)

    @pl.when(s < n_sp - 1)
    def _():
        out_line(out_ref, s, 1).start()

    @pl.when(s > 0)
    def _():
        out_line(out_ref, s, -1).start()

    for piece in range(2):
        start(remote(own(piece), spot(f, t, piece), side_sent.at[f, piece], side_landed.at[f, piece], other))
    for i, (a, b) in enumerate(
        (
            (own(0), spot(f, t, 0)),
            (own(1), spot(f, t, 1)),
            (weight_ref.at[f], block(s, f)),
            (decay_ref.at[f], decays_ref.at[f]),
            (out_ref, outs(s, f)),
        )
    ):
        copy = pltpu.make_async_copy(a, b, local_sem.at[i])
        copy.start()
        locals_.append(copy)

    for p in order:
        remote(weight_ref.at[p], block(s, p), weight_sent.at[0], weight_landed.at[p], {"fs": p}).wait_recv()
        send_line(block(s, p), s, p)

    for i in range(2):
        out_plane(out_ref, s, i).start()

    def arrived(owner, piece):
        view = spot(owner, t, piece)
        remote(view, view, norm_sent.at[0], norm_landed.at[owner, piece], {"fs": owner}).wait_recv()
        start(remote(view, view, side_sent.at[owner, piece], side_landed.at[owner, piece], other))

    def line_step(d):
        for g in (f,) + order:

            @pl.when(s - d >= 0)
            def _():
                line_copy(block(s - d, g), s - d, g, 1).wait_recv()

                @pl.when(s < n_sp - 1)
                def _():
                    line_copy(block(s - d, g), s - d, g, 1).start()

            @pl.when(s + d <= n_sp - 1)
            def _():
                line_copy(block(s + d, g), s + d, g, -1).wait_recv()

                @pl.when(s > 0)
                def _():
                    line_copy(block(s + d, g), s + d, g, -1).start()

    def out_step(d):
        for b, way, there, further in (
            (s - d, 1, s - d >= 0, s < n_sp - 1),
            (s + d, -1, s + d <= n_sp - 1, s > 0),
        ):

            @pl.when(there)
            def _():
                out_line(outs(b, f), b, way).wait_recv()

                @pl.when(further)
                def _():
                    out_line(outs(b, f), b, way).start()

                for i in range(2):
                    out_plane(outs(b, f), b, i).start()

    arrived(xn, 0)
    start(remote(spot(xn, t, 0), spot(xn, t, 0), relay_sent.at[0], norm_landed.at[xn, 0], {"fs": yn}))
    arrived(yn, 1)
    start(remote(spot(yn, t, 1), spot(yn, t, 1), relay_sent.at[1], norm_landed.at[yn, 1], {"fs": xn}))
    line_step(1)
    out_step(1)
    arrived(xn, 1)
    arrived(yn, 0)
    for d in range(2, n_sp - 1):
        line_step(d)
        out_step(d)
    arrived(dn, 0)
    arrived(dn, 1)
    if n_sp > 2:
        line_step(n_sp - 1)
        out_step(n_sp - 1)
    for p in order:
        remote(decay_ref.at[p], decays_ref.at[p], decay_sent.at[0], decay_landed.at[p], {"fs": p}).wait_recv()
    for owner in range(n_fs):
        for piece in range(2):
            view = spot(owner, 1 - t, piece)
            remote(view, view, side_sent.at[0, 0], side_landed.at[owner, piece], other).wait_recv()
    for copy in locals_:
        copy.wait()

    def out_landed(b, g):
        remote(outs(b, g), outs(b, g), out_relay_sent.at[0], out_plane_landed.at[b, g], {"fs": g}).wait_recv()

    for b in range(n_sp):
        g, onward = (xn, yn) if b < n_sp // 2 else (yn, xn)
        out_landed(b, g)
        start(
            remote(outs(b, g), outs(b, g), out_relay_sent.at[b], out_plane_landed.at[b, g], {"fs": onward})
        )

    tile = chunk
    tiles = 2 * half // tile

    @pl.loop(0, n_fs * tiles)
    def _(step):
        owner, at = step // tiles, pl.ds((step % tiles) * tile, tile)
        proj_ref[owner, at, :] = jnp.dot(
            normed_ref[owner, at, :], full_ref[...], preferred_element_type=jnp.float32
        ).astype(jnp.bfloat16)

    for b in range(n_sp):
        out_landed(b, yn if b < n_sp // 2 else xn)
        out_landed(b, dn)
    for copy in waits:
        copy.wait_send()
    for b in range(n_sp):
        for i in range(2):
            out_plane(outs(b, f), b, i).wait_send()

        @pl.when((s < n_sp - 1) & (b <= s))
        def _():
            out_line(outs(b, f), b, 1).wait_send()

        @pl.when((s > 0) & (b >= s))
        def _():
            out_line(outs(b, f), b, -1).wait_send()

    for b in range(n_sp):
        for g in range(n_fs):

            @pl.when((s < n_sp - 1) & (b <= s))
            def _():
                line_copy(block(b, g), b, g, 1).wait_send()

            @pl.when((s > 0) & (b >= s))
            def _():
                line_copy(block(b, g), b, g, -1).wait_send()


def gather_all(n_sp, half, pieces, decays, own_out):
    n_fs, rows, width = pieces.shape
    any_space = pl.BlockSpec(memory_space=pl.ANY)
    vmem = pl.BlockSpec(memory_space=pltpu.VMEM)
    dma = pltpu.SemaphoreType.DMA
    return pl.pallas_call(
        lambda *refs: gather_kernel(n_sp, *refs),
        out_shape=(
            jax.ShapeDtypeStruct((n_fs, 2 * half.shape[0], width), jnp.bfloat16),
            jax.ShapeDtypeStruct(decays.shape, jnp.float32),
            jax.ShapeDtypeStruct((n_sp * n_fs * rows, own_out.shape[1]), jnp.bfloat16),
        ),
        in_specs=[vmem] * 4,
        out_specs=(vmem, vmem, any_space),
        scratch_shapes=[
            pltpu.VMEM((n_fs, 2 * half.shape[0], half.shape[1]), jnp.bfloat16),
            pltpu.VMEM((n_sp * n_fs * rows, width), jnp.bfloat16),
            dma((4,)),
            dma((n_fs, 2)),
            dma((n_fs, 2)),
            dma((n_fs, 2)),
            dma((2,)),
            dma((3,)),
            dma((n_fs,)),
            dma((n_sp, n_fs)),
            dma((n_sp, n_fs)),
            dma((n_sp, n_fs)),
            dma((3,)),
            dma((n_fs,)),
            dma((5,)),
            dma((n_sp,)),
            dma((n_sp,)),
            dma((n_sp,)),
            dma((n_sp, 2)),
            dma((n_sp, n_fs)),
            dma((n_sp,)),
        ],
        compiler_params=pltpu.CompilerParams(collective_id=0, has_side_effects=True),
        cost_estimate=pl.CostEstimate(flops=0, bytes_accessed=200_000_000, transcendentals=0),
        name="gather_all",
    )(half, pieces, decays, own_out)


def swap_kernel(
    mixed_ref, weight_ref, same_ref, cross_ref, far_ref, sent, same_landed, cross_landed, weight_sems, local_sem
):
    f, t = lax.axis_index("fs"), lax.axis_index("tp")
    half = same_ref.shape[1]
    order = plane_partners(f)
    peers = [{"fs": p, "tp": q} for p in order for q in (t, 1 - t)] + [{"tp": 1 - t}]
    greet(peers)

    def mine(p, core):
        return mixed_ref.at[p, pl.ds(core * half, half), :]

    copies = []
    for i, p in enumerate((order[2], order[0], order[1])):
        copies.append(
            remote(mine(p, t), same_ref.at[f], sent.at[2 * i], same_landed.at[f], {"fs": p})
        )
        copies.append(
            remote(
                mine(p, 1 - t),
                cross_ref.at[f],
                sent.at[2 * i + 1],
                cross_landed.at[f],
                {"fs": p, "tp": 1 - t},
            )
        )
    copies.append(remote(mine(f, 1 - t), cross_ref.at[f], sent.at[6], cross_landed.at[f], {"tp": 1 - t}))
    for copy in copies:
        copy.start()
    weight = remote(weight_ref, far_ref, weight_sems.at[0], weight_sems.at[1], {"tp": 1 - t})
    weight.start()
    local = pltpu.make_async_copy(mine(f, t), same_ref.at[f], local_sem)
    local.start()
    for p in order:
        remote(same_ref.at[p], same_ref.at[p], sent.at[0], same_landed.at[p], {"fs": p}).wait_recv()
    for p in order + (f,):
        remote(cross_ref.at[p], cross_ref.at[p], sent.at[0], cross_landed.at[p], {"tp": 1 - t}).wait_recv()
    for copy in copies:
        copy.wait_send()
    local.wait()
    weight.wait()


def swap(mixed, weight):
    n_fs, rows, width = mixed.shape
    any_space = pl.BlockSpec(memory_space=pl.ANY)
    vmem = pl.BlockSpec(memory_space=pltpu.VMEM)
    dma = pltpu.SemaphoreType.DMA
    piece = jax.ShapeDtypeStruct((n_fs, rows // 2, width), jnp.bfloat16)
    return pl.pallas_call(
        swap_kernel,
        out_shape=(piece, piece, jax.ShapeDtypeStruct(weight.shape, weight.dtype)),
        in_specs=[vmem, any_space],
        out_specs=(vmem, vmem, any_space),
        scratch_shapes=[dma((7,)), dma((n_fs,)), dma((n_fs,)), dma((2,)), dma],
        compiler_params=pltpu.CompilerParams(collective_id=1, has_side_effects=True),
        cost_estimate=pl.CostEstimate(flops=0, bytes_accessed=60_000_000, transcendentals=0),
        name="swap",
    )(mixed, weight)


def pass_kernel(n_sp, state_ref, extra_ref, states_ref, extras_ref, sent, landed, local_sem):
    s = lax.axis_index("sp")
    greet([{"sp": (s + d) % n_sp} for d in range(1, n_sp)])

    def pair(source, here, owner, d):
        place = here.at[owner]
        slot = 0 if source is state_ref else 1
        return remote(source, place, sent.at[d, slot], landed.at[owner, slot], {"sp": (s + d) % n_sp})

    arrays = ((state_ref, states_ref), (extra_ref, extras_ref))
    for d in range(n_sp - 1, 0, -1):

        @pl.when(s + d < n_sp)
        def _():
            for source, here in arrays:
                pair(source, here, s, d).start()

    states_ref[n_sp - 1] = jnp.zeros_like(state_ref)
    extras_ref[n_sp - 1] = jnp.zeros_like(extra_ref)
    for k in range(n_sp - 1):

        @pl.when(k < s)
        def _():
            for source, here in arrays:
                pair(source, here, k, 1).wait_recv()

        @pl.when(k >= s)
        def _():
            states_ref[k] = jnp.zeros_like(state_ref)
            extras_ref[k] = jnp.zeros_like(extra_ref)

    for d in range(1, n_sp):

        @pl.when(s + d < n_sp)
        def _():
            for source, here in arrays:
                pair(source, here, s, d).wait_send()


def pass_on(n_sp, state, extra):
    vmem = pl.BlockSpec(memory_space=pltpu.VMEM)
    dma = pltpu.SemaphoreType.DMA
    return pl.pallas_call(
        lambda *refs: pass_kernel(n_sp, *refs),
        out_shape=(
            jax.ShapeDtypeStruct((n_sp,) + state.shape, state.dtype),
            jax.ShapeDtypeStruct((n_sp,) + extra.shape, extra.dtype),
        ),
        in_specs=[vmem] * 2,
        out_specs=(vmem, vmem),
        scratch_shapes=[dma((n_sp, 2)), dma((n_sp, 2)), dma],
        compiler_params=pltpu.CompilerParams(collective_id=2, has_side_effects=True),
        cost_estimate=pl.CostEstimate(flops=0, bytes_accessed=20_000_000, transcendentals=0),
        name="pass_on",
    )(state, extra)


def rotate_flat(values, cosine, sine):
    half_dim = values.shape[-1] // 2
    first = values[..., :half_dim].astype(jnp.float32)
    second = values[..., half_dim:].astype(jnp.float32)
    return jnp.concatenate([first * cosine - second * sine, first * sine + second * cosine], axis=-1)


def fast_shards(
    tokens,
    norm_gain,
    query_weight,
    key_weight,
    value_weight,
    gate_weight,
    conv_b_weight,
    conv_c_weight,
    conv_in_weight,
    conv_kernel,
    out_ret_weight,
    out_conv_weight,
    log_decay,
):
    n_sp, n_fs = lax.axis_size("sp"), lax.axis_size("fs")
    s, f, t = lax.axis_index("sp"), lax.axis_index("fs"), lax.axis_index("tp")
    tok_rows, model = tokens.shape[1:]
    half = tok_rows // 2
    blocks = tok_rows // BLOCK_LEN
    rows = query_weight.shape[0]
    inputs = lax.dynamic_slice_in_dim(tokens[0], t * half, half).astype(jnp.float32)
    normed = (
        inputs * lax.rsqrt(jnp.mean(inputs * inputs, axis=-1, keepdims=True) + EPSILON) * norm_gain
    ).astype(jnp.bfloat16)
    pieces = jnp.concatenate(
        [
            jnp.transpose(w.reshape(rows, n_fs, w.shape[1] // n_fs), (1, 0, 2))
            for w in (
                query_weight,
                key_weight,
                value_weight,
                gate_weight,
                conv_b_weight,
                conv_c_weight,
                conv_in_weight,
            )
        ],
        axis=-1,
    )
    own_out = jnp.concatenate([out_ret_weight, out_conv_weight], axis=-1)
    proj, decays, out_weight = gather_all(
        n_sp, normed, pieces, log_decay[0].reshape(n_fs, blocks, BLOCK_LEN), own_out
    )
    cuts = (KEY_DIM, 2 * KEY_DIM)
    q_raw, k_raw, wide = proj[..., : cuts[0]], proj[..., cuts[0] : cuts[1]], proj[..., cuts[1] :]
    values, ret_gate, gate_b, gate_c, conv_in = jnp.split(wide, 5, axis=-1)

    ordinal = (s * tok_rows + jnp.arange(tok_rows, dtype=jnp.int32)).astype(jnp.float32)
    frequency = 1.0 / ROPE_BASE ** jnp.linspace(0.0, 1.0, KEY_DIM // 2, dtype=jnp.float32)
    angles = ordinal[:, None] * frequency[None, :]
    cosine, sine = jnp.cos(angles), jnp.sin(angles)
    queries = rotate_flat(q_raw, cosine, sine).astype(jnp.bfloat16)
    keys = (rotate_flat(k_raw, cosine, sine) * KEY_DIM ** (-0.5)).astype(jnp.bfloat16)

    def cut(array):
        return array.reshape(n_fs, blocks, BLOCK_LEN, array.shape[-1])

    queries, keys, value_blocks = cut(queries), cut(keys), cut(values)
    cumulative = jnp.cumsum(decays, axis=-1)
    ending = cumulative[..., -1:]
    gaps = cumulative[..., :, None] - cumulative[..., None, :]
    causal = jnp.arange(BLOCK_LEN)[:, None] >= jnp.arange(BLOCK_LEN)[None, :]
    weighting = jnp.where(causal, jnp.exp(jnp.minimum(gaps, 0.0)), 0.0)
    decayed_keys = (keys.astype(jnp.float32) * jnp.exp(ending - cumulative)[..., None]).astype(
        jnp.bfloat16
    )
    block_kv = jnp.einsum(
        "bnjd,bnje->bnde", decayed_keys, value_blocks, preferred_element_type=jnp.float32
    )
    state = jnp.zeros_like(block_kv[:, 0])
    start = jnp.zeros_like(ending[:, 0])
    before, starts = [], []
    for n in range(blocks):
        before.append(state)
        starts.append(start)
        state = state * jnp.exp(ending[:, n])[..., None] + block_kv[:, n]
        start = start + ending[:, n]
    product = gate_c.astype(jnp.float32) * conv_in.astype(jnp.float32)
    halo = CONV_TAPS - 1
    extra = jnp.concatenate(
        [
            product[:, tok_rows - halo :],
            jnp.broadcast_to(start[..., None], (n_fs, 8 - halo, product.shape[-1])),
        ],
        axis=1,
    )
    all_states, extras = pass_on(n_sp, state.astype(jnp.bfloat16), extra)
    state_in = jnp.zeros_like(state)
    rim = jnp.zeros_like(product[:, :halo])
    for k in range(n_sp - 1):
        part, total = all_states[k].astype(jnp.float32), extras[k, :, halo : halo + 1, :1]
        state_in = jnp.where(k < s, state_in * jnp.exp(total) + part, state_in)
        rim = jnp.where(k == s - 1, extras[k, :, :halo], rim)

    raw = jnp.einsum("bnid,bnjd->bnij", queries, keys, preferred_element_type=jnp.float32)
    scores = (raw * weighting).astype(jnp.bfloat16)
    intra = jnp.einsum("bnij,bnje->bnie", scores, value_blocks, preferred_element_type=jnp.float32)
    decayed_queries = (queries.astype(jnp.float32) * jnp.exp(cumulative)[..., None]).astype(
        jnp.bfloat16
    )
    full_states = (
        jnp.stack(before, axis=1) + jnp.exp(jnp.stack(starts, axis=1))[..., None] * state_in[:, None]
    )
    cross = jnp.einsum(
        "bnid,bnde->bnie",
        decayed_queries,
        full_states.astype(jnp.bfloat16),
        preferred_element_type=jnp.float32,
    )
    output = intra + cross
    output = output * lax.rsqrt(jnp.mean(output * output, axis=-1, keepdims=True) + EPSILON)
    output = output.reshape(n_fs, tok_rows, values.shape[-1])
    ret_out = (output * jax.nn.silu(ret_gate.astype(jnp.float32))).astype(jnp.bfloat16)

    padded = jnp.concatenate([rim, product], axis=1)
    width = product.shape[-1]
    taps = lax.dynamic_slice_in_dim(conv_kernel, f * width, width, axis=1)
    convolved = sum(taps[k] * padded[:, k : k + tok_rows] for k in range(CONV_TAPS))
    conv_out = (gate_b.astype(jnp.float32) * convolved).astype(jnp.bfloat16)

    same, cross_core, far_weight = swap(jnp.concatenate([ret_out, conv_out], axis=-1), out_weight)

    def spread(piece):
        parts = piece.reshape(n_fs, half, 2, width)
        return jnp.transpose(parts, (1, 2, 0, 3)).reshape(half, 2 * n_fs * width)

    def project(piece, weight):
        return lax.dot_general(
            spread(piece), weight, (((1,), (1,)), ((), ())), preferred_element_type=jnp.float32
        )

    mixed = project(same, out_weight) + project(cross_core, far_weight)
    return mixed.astype(jnp.bfloat16)[None]


def select(mesh):
    def chosen(*arrays):
        heads, conv_width = arrays[12].shape[1], arrays[9].shape[1]
        n_sp, n_fs, n_tp = (mesh.shape[name] for name in ("sp", "fs", "tp"))
        fits = n_fs == 4 and n_tp == 2 and n_sp > 1 and heads == n_fs
        fits = fits and conv_width == n_fs * VALUE_DIM and arrays[0].shape[1] % (2 * BLOCK_LEN) == 0
        return (fast_shards if fits else shards)(*arrays)

    return chosen


def solution(mesh):
    in_specs = (
        P("fs", "sp", None),
        P(),
        P(("sp", "fs"), "tp"),
        P(("sp", "fs"), "tp"),
        P(("sp", "fs"), "tp"),
        P(("sp", "fs"), "tp"),
        P(("sp", "fs"), "tp"),
        P(("sp", "fs"), "tp"),
        P(("sp", "fs"), "tp"),
        P(None, "tp"),
        P(("sp", "fs"), "tp"),
        P(("sp", "fs"), "tp"),
        P("fs", "tp", "sp"),
    )
    out_specs = P("fs", ("sp", "tp"), None)
    return jax.shard_map(select(mesh), mesh=mesh, in_specs=in_specs, out_specs=out_specs, check_vma=False)
```

profile of v0, /device:TPU:0, one launch (start us, length us, event | category | flops | bytes accessed | tf_op | source)
XLA Modules:
  0.0 205.6 jit_solution(7047235231887003056)
XLA Ops:
  0.0 1.8 fusion
  1.9 3.1 %fusion.2.refs_0_ = bf16[384,2048]{1,0:T(8,128)(2,1)} fusion(f32[2048]{0:T(1024)S(1)} %copy-done.20, f32[384]{0:T(512)S(1)} %add_rsqrt_fusion.1, bf16[1,768,2048]{2,1,0:T(8,128)(2,1)} %param.13, s32[]{:T(128)S(6)} %select_n.67), kind=kLoop, calls=%fused_computation.4 | loop fusion | flops 3145728 | bytes 3155460 | tf_op jit(solution)/shard_map/convert_element_type | solution.py:679
  6.9 1.2 concatenate.46.refs_1_
  9.4 108.1 %gather_all.1 = (bf16[4,768,768]{2,1,0:T(8,128)(2,1)}, f32[4,6,128]{2,1,0:T(8,128)}, bf16[2048,1024]{1,0:T(8,128)(2,1)}) custom-call(bf16[384,2048]{1,0:T(8,128)(2,1)} %fusion.2.refs_0_, bf16[4,128,768]{2,1,0:T(8,128)(2,1)} %concatenate.46.refs_1_, f32[4,6,128]{2,1,0:T(8,128)} %reshape_squeeze.3.refs_2_, bf16[128,1024]{1,0:T(8,128)(2,1)} %pad_maximum_fusion.3.refs_3_), custom_call_target="tpu_custom_call" | custom-call | bytes 200000000 | tf_op jit(solution)/shard_map/gather_all/pallas_call | solution.py:492
  117.5 2.2 %reduce_window_sum.11 = f32[4,6,128]{2,1,0:T(8,128)S(1)} reduce-window(f32[4,6,128]{2,1,0:T(8,128)} %get-tuple-element.14, f32[]{:T(128)} %constant.23.clone.1), window={size=1x1x128 pad=0_0x0_0x127_0}, to_apply=%region_1.2 | reduce-window | flops 390144 | bytes 24580 | tf_op jit(solution)/shard_map/jit(cumsum)/reduce_window_sum | solution.py:714
  120.7 1.4 multiply_cosine_fusion
  122.1 5.1 %fusion.11 = (bf16[4,768,32]{2,1,0:T(8,128)(2,1)}, bf16[4,768,32]{2,1,0:T(8,128)(2,1)}, f32[4,768,32]{2,1,0:T(8,128)S(1)}, f32[4,768,32]{2,1,0:T(8,128)S(1)}) fusion(f32[768,32]{1,0:T(8,128)S(1)} %get-tuple-element.51, f32[768,32]{1,0:T(8,128)S(1)} %get-tuple-element.50, bf16[4,768,768]{2,1,0:T(8,128)(2,1)} %get-tuple-element.13), kind=kLoop, calls=%fused_computation.26 | loop fusion | flops 1769472 | bytes 2162688 | tf_op jit(solution)/shard_map/convert.7
  127.2 2.1 %copy.40 = bf16[4,6,128,32]{2,3,1,0:T(8,128)(2,1)} copy(bf16[4,6,128,32]{3,2,1,0:T(8,128)(2,1)} %bitcast.101) | data formatting | bytes 393216 | tf_op jit(solution)/shard_map/concatenate | solution.py:652
  129.3 2.1 %copy.39 = bf16[4,6,128,32]{2,3,1,0:T(8,128)(2,1)} copy(bf16[4,6,128,32]{3,2,1,0:T(8,128)(2,1)} %bitcast.100) | data formatting | bytes 393216 | tf_op jit(solution)/shard_map/concatenate | solution.py:652
  132.0 2.1 %split.15 = bf16[4,768,128]{2,1,0:T(8,128)(2,1)} slice(bf16[4,768,768]{2,1,0:T(8,128)(2,1)} %get-tuple-element.13), slice={[0:4], [0:768], [128:256]} | slice | bytes 1572864 | tf_op jit(solution)/shard_map/split | solution.py:701
  137.8 0.9 fusion.34.refs_0_
  138.8 1.6 convert_multiply_fusion.11
  141.0 6.5 %pass_on.1 = (bf16[4,4,64,128]{3,2,1,0:T(8,128)(2,1)}, f32[4,4,8,128]{3,2,1,0:T(8,128)}) custom-call(bf16[4,64,128]{2,1,0:T(8,128)(2,1)} %fusion.34.refs_0_, f32[4,8,128]{2,1,0:T(8,128)} %pad_maximum_fusion.7.refs_1_), custom_call_target="tpu_custom_call" | custom-call | bytes 20000000 | tf_op jit(solution)/shard_map/pass_on/pallas_call | solution.py:633
  147.5 1.4 multiply_reduce_fusion.1
  148.9 1.7 fusion.35
  151.3 2.8 %fusion.29 = f32[4,6,128,128]{3,2,1,0:T(8,128)} fusion(f32[4,6,128]{2,1,0:T(8,128)} %get-tuple-element.48, bf16[4,6,128,32]{2,3,1,0:T(8,128)(2,1)S(1)} %copy-done.5, bf16[4,6,128,32]{2,3,1,0:T(8,128)(2,1)S(1)} %copy-done.6, f32[4,6,64,128]{3,2,0,1:T(8,128)} %copy-done.3, f32[4,64,128]{2,1,0:T(8,128)} %fusion.35, f32[4,6]{0,1:T(8,128)S(1)} %exp.105), kind=kOutput, calls=%fused_computation.57 | convolution fusion | flops 52101120 | bytes 2895968 | tf_op jit(solution)/shard_map/bnid,bnde->bnie/dot_general | solution.py:759
  154.8 4.4 %multiply_reduce_fusion = (f32[4,6,128]{2,1,0:T(8,128)}, f32[4,6,128,128]{3,2,1,0:T(8,128)}) fusion(f32[4,6,128,128]{3,2,1,0:T(8,128)} %fusion.29, bf16[4,6,128,128]{3,2,1,0:T(8,128)(2,1)S(1)} %bitcast.103, f32[4,6,128]{2,1,0:T(8,128)} %copy-done.7, pred[128,128]{1,0:T(8,128)(4,1)} %iota_compare_fusion, bf16[4,6,128,32]{2,3,1,0:T(8,128)(2,1)S(1)} %copy-done.5, ...), kind=kOutput, calls=%fused_computation.38 | convolution fusion | flops 155513856 | bytes 5152768 | tf_op jit(solution)/shard_map/bnij,bnje->bnie/dot_general | solution.py:752
  159.9 1.9 broadcast_multiply_fusion
  162.6 2.5 %fusion.21 = (bf16[4,768,128]{2,1,0:T(8,128)(2,1)S(1)}, bf16[4,768,128]{2,1,0:T(8,128)(2,1)S(1)}) fusion(f32[4,6,128,128]{3,2,1,0:T(8,128)S(1)} %broadcast_multiply_fusion, bf16[4,768,768]{2,1,0:T(8,128)(2,1)} %get-tuple-element.13, f32[4,768,128]{2,1,0:T(8,128)S(1)} %convert_multiply_fusion.11, f32[128]{0:T(128)S(1)} %get-tuple-element.53, ...), kind=kLoop, calls=%fused_computation.41 | loop fusion | flops 6684672 | bytes 6297088 | tf_op jit(solution)/shard_map/convert_element_type | solution.py:768
  165.1 1.3 pad_maximum_fusion.1.mixed_ref
  166.4 23.5 %swap.1 = (bf16[4,384,256]{2,1,0:T(8,128)(2,1)}, bf16[4,384,256]{2,1,0:T(8,128)(2,1)}, bf16[2048,1024]{1,0:T(8,128)(2,1)}) custom-call(bf16[4,768,256]{2,1,0:T(8,128)(2,1)} %pad_maximum_fusion.1.mixed_ref, bf16[2048,1024]{1,0:T(8,128)(2,1)} %get-tuple-element.17.weight_ref), custom_call_target="tpu_custom_call" | custom-call | bytes 60000000 | tf_op jit(solution)/shard_map/swap/pallas_call | solution.py:579
  189.9 2.0 reshape.345
  192.7 5.8 %fusion.61 = f32[384,2048]{1,0:T(8,128)} fusion(bf16[384,1024]{0,1:T(8,128)(2,1)S(1)} %bitcast.105, bf16[2048,1024]{1,0:T(8,128)(2,1)} %get-tuple-element.17.weight_ref), kind=kOutput, calls=%fused_computation.131 | convolution fusion | flops 1610612736 | bytes 8126464 | tf_op jit(solution)/shard_map/dot_general | solution.py:783
  199.4 6.2 %fusion.3 = bf16[1,384,2048]{2,1,0:T(8,128)(2,1)} fusion(f32[384,2048]{1,0:T(8,128)} %fusion.61, bf16[384,1024]{0,1:T(8,128)(2,1)S(1)} %bitcast.104, bf16[2048,1024]{1,0:T(8,128)(2,1)} %get-tuple-element.20), kind=kOutput, calls=%fused_computation.6 | convolution fusion | flops 1612185600 | bytes 9699328 | tf_op jit(solution)/shard_map/dot_general | solution.py:783
  (89 shorter events, 13.5 us)
Async XLA Ops:
  0.0 161.7 %copy-start = (f32[3,512]{1,0:T(4,128)S(1)}, f32[3,512]{1,0:T(4,128)}, u32[]{:S(2)}) copy-start(f32[3,512]{1,0:T(4,128)} %param.22) | copy-start | bytes 18436
  0.0 1.8 copy-start.20
  1.8 3.1 %copy-start.17 = (bf16[128,256]{1,0:T(8,128)(2,1)S(1)}, bf16[128,256]{1,0:T(8,128)(2,1)}, u32[]{:S(2)}) copy-start(bf16[128,256]{1,0:T(8,128)(2,1)} %param.15) | copy-start | bytes 196612
  1.9 3.4 %copy-start.18 = (bf16[128,256]{1,0:T(8,128)(2,1)S(1)}, bf16[128,256]{1,0:T(8,128)(2,1)}, u32[]{:S(2)}) copy-start(bf16[128,256]{1,0:T(8,128)(2,1)} %param.16) | copy-start | bytes 196612
  1.9 3.6 %copy-start.9 = (bf16[128,512]{1,0:T(8,128)(2,1)S(1)}, bf16[128,512]{1,0:T(8,128)(2,1)}, u32[]{:S(2)}) copy-start(bf16[128,512]{1,0:T(8,128)(2,1)} %param.17) | copy-start | bytes 393220
  1.9 3.9 %copy-start.10 = (bf16[128,512]{1,0:T(8,128)(2,1)S(1)}, bf16[128,512]{1,0:T(8,128)(2,1)}, u32[]{:S(2)}) copy-start(bf16[128,512]{1,0:T(8,128)(2,1)} %param.18) | copy-start | bytes 393220
  4.9 1.1 copy-start.11
  4.9 1.4 copy-start.12
  4.9 1.7 copy-start.13
  6.2 1.9 copy-start.19
  6.2 2.5 %copy-start.14 = (bf16[128,512]{1,0:T(8,128)(2,1)S(1)}, bf16[128,512]{1,0:T(8,128)(2,1)}, u32[]{:S(2)}) copy-start(bf16[128,512]{1,0:T(8,128)(2,1)} %param.24) | copy-start | bytes 393220
  6.2 2.5 %copy-start.15 = (bf16[128,512]{1,0:T(8,128)(2,1)S(1)}, bf16[128,512]{1,0:T(8,128)(2,1)}, u32[]{:S(2)}) copy-start(bf16[128,512]{1,0:T(8,128)(2,1)} %param.23) | copy-start | bytes 393220
  119.7 2.4 %copy-start.7 = (f32[4,6,128]{2,1,0:T(8,128)}, f32[4,6,128]{2,1,0:T(8,128)S(1)}, u32[]{:S(2)}) copy-start(f32[4,6,128]{2,1,0:T(8,128)S(1)} %reduce_window_sum.11) | copy-start | bytes 36868
  134.5 1.1 copy-start.1
  134.5 1.1 copy-start.16
  135.7 0.7 copy-start.8
  135.7 1.6 copy-start.2
  137.8 2.6 %copy-start.3 = (f32[4,6,64,128]{3,2,0,1:T(8,128)}, f32[4,6,64,128]{3,2,0,1:T(8,128)S(1)}, u32[]{:S(2)}) copy-start(f32[4,6,64,128]{3,2,0,1:T(8,128)S(1)} %add_dynamic-update-slice_fusion) | copy-start | bytes 2359300
  138.7 12.6 %copy-start.5 = (bf16[4,6,128,32]{2,3,1,0:T(8,128)(2,1)S(1)}, bf16[4,6,128,32]{2,3,1,0:T(8,128)(2,1)}, u32[]{:S(2)}) copy-start(bf16[4,6,128,32]{2,3,1,0:T(8,128)(2,1)} %copy.40) | copy-start | bytes 589828
  138.8 12.6 %copy-start.6 = (bf16[4,6,128,32]{2,3,1,0:T(8,128)(2,1)S(1)}, bf16[4,6,128,32]{2,3,1,0:T(8,128)(2,1)}, u32[]{:S(2)}) copy-start(bf16[4,6,128,32]{2,3,1,0:T(8,128)(2,1)} %copy.39) | copy-start | bytes 589828
  192.7 5.8 %copy-start.4 = (bf16[4,384,256]{2,1,0:T(8,128)(2,1)S(1)}, bf16[4,384,256]{2,1,0:T(8,128)(2,1)}, u32[]{:S(2)}) copy-start(bf16[4,384,256]{2,1,0:T(8,128)(2,1)} %get-tuple-element.19) | copy-start | bytes 2359300
where the time goes:
time: 207 us; the launch traced here: 206 us
  Pallas kernels  138 us (67%)
  other arithmetic  30.5 us (15%)
  matrix products  19.5 us (9%)
  local copies, waits for them, and re-layouts  17 us (8%)
    pallas_call x1, Pallas kernels, gather_all(): pl.pallas_call(lambda *refs: gather_kernel(n_sp, *refs), out_shape=(jax.S...  108 us
    pallas_call x1, Pallas kernels, swap(): pl.pallas_call(swap_kernel, out_shape=(piece, piece, jax.ShapeDtypeStruct...  23.5 us
    dot_general x2, matrix products, project(): lax.dot_general(spread(piece), weight, (((1,), (1,)), ((), ())), preferre...  12 us
    pallas_call x1, Pallas kernels, pass_on(): pl.pallas_call(lambda *refs: pass_kernel(n_sp, *refs), out_shape=(jax.Sha...  6.55 us
    another operation x1, other arithmetic  5.12 us
    concatenate x4, local copies, waits for them, and re-layouts, rotate_flat(): jnp.concatenate([first * cosine - second * sine, first * sine + second *...  5 us
    dot_general x1, matrix products, fast_shards(): jnp.einsum('bnij,bnje->bnie', scores, value_blocks, preferred_element_typ...  4.37 us

commit v1 on v0

v1 whole, which is shorter than its diff:
```python
import jax
import numpy as np
import jax.numpy as jnp
from jax import lax
from jax.experimental import pallas as pl
from jax.experimental.pallas import tpu as pltpu
from jax.sharding import PartitionSpec as P

KEY_DIM = 64
VALUE_DIM = 128
CONV_TAPS = 3
BLOCK_LEN = 128


EPSILON = 1e-06
ROPE_BASE = 10000.0


def entering(x, axis, combine, identity):
    length, here = (lax.axis_size(axis), lax.axis_index(axis))
    everything = jax.tree.map(
        lambda part, kind: lax.all_gather(part.astype(kind), axis), x, (jnp.bfloat16, jnp.bfloat16)
    )
    start = jax.tree.map(
        lambda part, zero: jnp.broadcast_to(jnp.asarray(zero, part.dtype), part.shape), x, identity
    )

    def lap(k, before):
        reached = k < here
        new = combine(
            before, jax.tree.map(lambda part, own: part[k].astype(own.dtype), everything, x)
        )
        return jax.tree.map(lambda a, b: jnp.where(reached, a, b), new, before)

    return lax.fori_loop(0, length, lap, start)


def passed_along(value, axis, steps):
    count = lax.axis_size(axis)
    first, last = (max(0, -steps), min(count, count - steps))
    return lax.ppermute(value, axis, [(source, source + steps) for source in range(first, last)])


def rotate(values, token_ordinal):
    half_dim = values.shape[-1] // 2
    frequency = 1.0 / ROPE_BASE ** jnp.linspace(0.0, 1.0, half_dim, dtype=jnp.float32)
    angles = token_ordinal[:, None] * frequency[None, :]
    cosine_table = jnp.cos(angles)[:, None, :]
    sine_table = jnp.sin(angles)[:, None, :]
    first = values[..., :half_dim].astype(jnp.float32)
    second = values[..., half_dim:].astype(jnp.float32)
    return jnp.concatenate(
        [first * cosine_table - second * sine_table, first * sine_table + second * cosine_table],
        axis=-1,
    )


def make_adder(normed, contracted, pieces):
    updated = []
    for member in range(len(pieces)):
        portion = pieces[member]
        if member < contracted:
            updated.append(jnp.dot(normed, portion, preferred_element_type=jnp.float32))
        else:
            updated.append(portion)
    return tuple(updated)


def retention_local(projections, decays, token_ordinal):
    tok_rows = token_ordinal.shape[0]
    head_count = decays.shape[0]
    blocks = tok_rows // BLOCK_LEN
    query_raw = projections[0].reshape(tok_rows, head_count, KEY_DIM)
    key_raw = projections[1].reshape(tok_rows, head_count, KEY_DIM)
    queries = rotate(query_raw, token_ordinal).astype(jnp.bfloat16)
    lookup_matrix_lines = (rotate(key_raw, token_ordinal) * KEY_DIM ** (-0.5)).astype(jnp.bfloat16)
    value_proj = projections[2].reshape(tok_rows, head_count, VALUE_DIM)

    def split_blocks(array):
        shaped = array.reshape(blocks, BLOCK_LEN, head_count, array.shape[-1])
        return jnp.transpose(shaped, (0, 2, 1, 3))

    query_blocks = split_blocks(queries)
    key_blocks = split_blocks(lookup_matrix_lines)
    value_blocks = split_blocks(value_proj)
    decay_blocks = jnp.transpose(decays.reshape(head_count, blocks, BLOCK_LEN), (1, 0, 2))
    cumulative = jnp.cumsum(decay_blocks, axis=-1)
    ending = cumulative[..., -1:]
    decay_gaps = cumulative[..., :, None] - cumulative[..., None, :]
    causal = jnp.arange(BLOCK_LEN)[:, None] >= jnp.arange(BLOCK_LEN)[None, :]
    weighting = jnp.where(causal, jnp.exp(jnp.minimum(decay_gaps, 0.0)), 0.0)
    raw_scores = jnp.einsum(
        "nhid,nhjd->nhij", query_blocks, key_blocks, preferred_element_type=jnp.float32
    )
    scores = (raw_scores * weighting).astype(jnp.bfloat16)
    intra_out = jnp.einsum(
        "nhij,nhje->nhie", scores, value_blocks, preferred_element_type=jnp.float32
    )
    decayed_keys = (
        key_blocks.astype(jnp.float32) * jnp.exp(ending - cumulative)[..., None]
    ).astype(jnp.bfloat16)
    decayed_queries = (query_blocks.astype(jnp.float32) * jnp.exp(cumulative)[..., None]).astype(
        jnp.bfloat16
    )
    block_kv = jnp.einsum(
        "nhjd,nhje->nhde", decayed_keys, value_blocks, preferred_element_type=jnp.float32
    )
    block_ends = ending[..., 0]

    def advance(state_now, step_in):
        kv_block, total = step_in
        return (state_now * jnp.exp(total)[:, None, None] + kv_block, state_now)

    start_state = jnp.zeros((head_count, KEY_DIM, VALUE_DIM), jnp.float32)
    end_state, before_local = lax.scan(advance, start_state, (block_kv, block_ends))
    device_total = jnp.sum(block_ends, axis=0)
    return (intra_out, decayed_queries, before_local, block_ends, end_state, device_total)


def combine(earlier, later):
    return (earlier[0] * jnp.exp(later[1])[:, None, None] + later[0], earlier[1] + later[1])


def carried(end_state, device_total):
    identity = (jnp.zeros_like(end_state), jnp.zeros_like(device_total))
    state_in, _ = entering((end_state, device_total), "sp", combine, identity)
    return state_in


def retention_finish(local_parts, state_in, gate_proj):
    intra_out, decayed_queries, before_local, block_ends, end_state, device_total = local_parts
    starts = jnp.cumsum(block_ends, axis=0) - block_ends
    full_states = before_local + jnp.exp(starts)[:, :, None, None] * state_in[None]
    cross = jnp.einsum(
        "nhid,nhde->nhie",
        decayed_queries,
        full_states.astype(jnp.bfloat16),
        preferred_element_type=jnp.float32,
    )
    output = intra_out + cross
    output = output * lax.rsqrt(jnp.mean(output * output, axis=-1, keepdims=True) + EPSILON)
    tok_rows = gate_proj.shape[0]
    output = jnp.transpose(output, (0, 2, 1, 3)).reshape(tok_rows, gate_proj.shape[1])
    return (output * jax.nn.silu(gate_proj.astype(jnp.float32))).astype(jnp.bfloat16)


def convolve(conv_proj, conv_kernel):
    gate_b, gate_c, conv_input = conv_proj
    tok_rows = gate_b.shape[0]
    product = gate_c.astype(jnp.float32) * conv_input.astype(jnp.float32)
    rim_rows = passed_along(product[tok_rows - (CONV_TAPS - 1) :], "sp", 1)
    padded = jnp.concatenate([rim_rows, product], axis=0)
    convolved = jnp.zeros_like(product)
    for tap_index in range(CONV_TAPS):
        convolved = convolved + conv_kernel[tap_index] * padded[tap_index : tap_index + tok_rows]
    return (gate_b.astype(jnp.float32) * convolved).astype(jnp.bfloat16)


def shards(
    tokens,
    norm_gain,
    query_weight,
    key_weight,
    value_weight,
    gate_weight,
    conv_b_weight,
    conv_c_weight,
    conv_in_weight,
    conv_kernel,
    out_ret_weight,
    out_conv_weight,
    log_decay,
):
    inputs = tokens[0].astype(jnp.float32)
    tok_rows = inputs.shape[0]
    normed = (
        inputs * lax.rsqrt(jnp.mean(inputs * inputs, axis=-1, keepdims=True) + EPSILON) * norm_gain
    ).astype(jnp.bfloat16)
    token_ordinal = (
        lax.axis_index("sp") * tok_rows + jnp.arange(tok_rows, dtype=jnp.int32)
    ).astype(jnp.float32)
    decays = log_decay[0]
    gathered = make_adder(
        normed,
        7,
        (
            lax.all_gather(query_weight, ("sp", "fs"), axis=0, tiled=True),
            lax.all_gather(key_weight, ("sp", "fs"), axis=0, tiled=True),
            lax.all_gather(value_weight, ("sp", "fs"), axis=0, tiled=True),
            lax.all_gather(gate_weight, ("sp", "fs"), axis=0, tiled=True),
            lax.all_gather(conv_b_weight, ("sp", "fs"), axis=0, tiled=True),
            lax.all_gather(conv_c_weight, ("sp", "fs"), axis=0, tiled=True),
            lax.all_gather(conv_in_weight, ("sp", "fs"), axis=0, tiled=True),
            lax.all_gather(out_ret_weight, ("sp", "fs"), axis=0, tiled=True),
            lax.all_gather(out_conv_weight, ("sp", "fs"), axis=0, tiled=True),
        ),
    )
    ret_proj = [member.astype(jnp.bfloat16) for member in gathered[:4]]
    local_parts = retention_local(ret_proj, decays, token_ordinal)
    state_in = carried(local_parts[4], local_parts[5])
    conv_proj = [member.astype(jnp.bfloat16) for member in gathered[4:7]]
    full_ret, full_conv = (gathered[7], gathered[8])
    conv_out = convolve(conv_proj, conv_kernel)
    ret_out = retention_finish(local_parts, state_in, ret_proj[3])
    partial_value = lax.dot_general(
        ret_out, full_ret, (((1,), (1,)), ((), ())), preferred_element_type=jnp.float32
    )
    mixed = lax.psum_scatter(
        (
            partial_value
            + lax.dot_general(
                conv_out, full_conv, (((1,), (1,)), ((), ())), preferred_element_type=jnp.float32
            )
        ).astype(jnp.bfloat16),
        "tp",
        scatter_dimension=0,
        tiled=True,
    )
    return mixed[None]


MESH_IDS = pl.DeviceIdType.MESH
OUT_CUT = 2
OUT_TILE = 512


def remote(source, target, sent, landed, device):
    return pltpu.make_async_remote_copy(
        src_ref=source,
        dst_ref=target,
        send_sem=sent,
        recv_sem=landed,
        device_id=device,
        device_id_type=MESH_IDS,
    )


def greet(peers):
    barrier = pltpu.get_barrier_semaphore()
    for peer in peers:
        pl.semaphore_signal(barrier, inc=1, device_id=peer, device_id_type=MESH_IDS)
    pl.semaphore_wait(barrier, len(peers))


def plane_partners(f):
    x, y = f % 2, f // 2
    return y * 2 + (1 - x), (1 - y) * 2 + x, 3 - f


def mixer_kernel(
    n_sp,
    tokens_ref,
    gain_ref,
    query_ref,
    key_ref,
    value_ref,
    gate_ref,
    conv_b_ref,
    conv_c_ref,
    conv_in_ref,
    taps_ref,
    out_ret_ref,
    out_conv_ref,
    decay_ref,
    near_cos_ref,
    near_sin_ref,
    base_ref,
    out_ref,
    raw_ref,
    normed_ref,
    pieces_ref,
    heads_ref,
    full_ref,
    outs_ref,
    decay_piece_ref,
    decays_ref,
    cos_ref,
    sin_ref,
    proj_ref,
    intra_ref,
    decayed_ref,
    before_ref,
    starts_ref,
    product_ref,
    state_ref,
    state_piece_ref,
    states_ref,
    extra_piece_ref,
    extras_ref,
    mixed_ref,
    merged_ref,
    part_ref,
    far_ref,
    local_sem,
    weight_sent,
    weight_landed,
    decay_sent,
    decay_landed,
    norm_sent,
    norm_landed,
    side_sent,
    side_landed,
    relay_sent,
    up_sent,
    down_sent,
    line_landed,
    wide_sent,
    wide_landed,
    wide_up_sent,
    wide_down_sent,
    wide_line_landed,
    slim_up_sent,
    slim_down_sent,
    slim_line_landed,
    slim_sent,
    slim_landed,
    slim_relay_sent,
    state_sent,
    state_landed,
    mixed_sent,
    mixed_landed,
    part_sent,
    part_landed,
):
    f32, bf16 = jnp.float32, jnp.bfloat16
    s, f, t = lax.axis_index("sp"), lax.axis_index("fs"), lax.axis_index("tp")
    xn, yn, dn = plane_partners(f)
    order = (xn, yn, dn)
    other = {"tp": 1 - t}
    n_fs, tok, model = normed_ref.shape
    half = tok // 2
    chunk = half // 2
    rows = query_ref.shape[0]
    blocks = tok // BLOCK_LEN
    lanes = 2 * KEY_DIM
    pair = 2 * VALUE_DIM
    halo = CONV_TAPS - 1
    cut = rows // OUT_CUT

    def lane(index, width):
        return pl.ds(pl.multiple_of(index * width, width), width)

    waits = []
    guarded = []

    def start(copy):
        copy.start()
        waits.append(copy)

    def start_when(condition, copy):
        @pl.when(condition)
        def _():
            copy.start()

        guarded.append((condition, copy))

    count = [0]

    def fetch(source, target):
        copy = pltpu.make_async_copy(source, target, local_sem.at[count[0]])
        count[0] += 1
        copy.start()
        return copy

    def block(b, g):
        return full_ref.at[pl.ds((b * n_fs + g) * rows, rows), :]

    def wide(b, g):
        return outs_ref.at[pl.ds((b * n_fs + g) * rows, cut), :]

    def slim(b, g):
        return outs_ref.at[pl.ds((b * n_fs + g) * rows + cut, rows - cut), :]

    head_loads = [fetch(query_ref, heads_ref.at[0]), fetch(key_ref, heads_ref.at[1])]
    wide_weights = (value_ref, gate_ref, conv_b_ref, conv_c_ref, conv_in_ref)
    piece_loads = []
    for p in range(n_fs):
        for j, weight in enumerate(wide_weights):
            piece_loads.append(
                fetch(
                    weight.at[:, pl.ds(p * VALUE_DIM, VALUE_DIM)],
                    pieces_ref.at[p, :, pl.ds(lanes + j * VALUE_DIM, VALUE_DIM)],
                )
            )
    own_loads = [
        fetch(
            weight.at[:, lane(f, VALUE_DIM)],
            full_ref.at[pl.ds((s * n_fs + f) * rows, rows), pl.ds(lanes + j * VALUE_DIM, VALUE_DIM)],
        )
        for j, weight in enumerate(wide_weights)
    ]
    raw_loads = [
        fetch(
            tokens_ref.at[0, pl.ds(t * half + i * chunk, chunk), :], raw_ref.at[pl.ds(i * chunk, chunk), :]
        )
        for i in range(2)
    ]
    out_loads = []
    for g in range(n_fs):
        for j, weight in enumerate((out_ret_ref, out_conv_ref)):
            out_loads.append(
                fetch(
                    weight.at[:, pl.ds(g * VALUE_DIM, VALUE_DIM)],
                    outs_ref.at[
                        pl.ds((s * n_fs + f) * rows, rows), pl.ds(g * pair + j * VALUE_DIM, VALUE_DIM)
                    ],
                )
            )
    table_loads = [fetch(near_cos_ref, cos_ref), fetch(near_sin_ref, sin_ref)]

    peers = [{"fs": p} for p in order] + [other]
    peers += [{"sp": (s + d) % n_sp} for d in range(1, n_sp)]
    greet(peers)

    for copy in head_loads:
        copy.wait()
    for p in range(n_fs):
        own = pl.ds(p * KEY_DIM, KEY_DIM)
        pieces_ref[p, :, 0:lanes] = jnp.concatenate([heads_ref[0, :, own], heads_ref[1, :, own]], axis=-1)
    full_ref[pl.ds((s * n_fs + f) * rows, rows), 0:lanes] = pieces_ref[f, :, 0:lanes]
    decay_piece_ref[...] = jnp.zeros_like(decay_piece_ref)
    for p in range(n_fs):
        for n in range(blocks):
            decay_piece_ref[p, n : n + 1, :] = decay_ref[0, p : p + 1, n * BLOCK_LEN : (n + 1) * BLOCK_LEN]
    decays_ref[f] = decay_piece_ref[f]
    for copy in piece_loads:
        copy.wait()
    for i, p in enumerate(order):
        start(remote(pieces_ref.at[p], block(s, f), weight_sent.at[i], weight_landed.at[f], {"fs": p}))

    def line(view, up, down, landed):
        def copy(source, way):
            return remote(source, view, up if way == 1 else down, landed, {"sp": s + way})

        def send():
            start_when(s < n_sp - 1, copy(view, 1))
            start_when(s > 0, copy(view, -1))

        def step(d, b, way, then):
            there = (s - d >= 0) if way == 1 else (s + d <= n_sp - 1)
            further = there & ((s < n_sp - 1) if way == 1 else (s > 0))

            @pl.when(there)
            def _():
                copy(view, way).wait_recv()

            start_when(further, copy(view, way))
            if then is not None:
                then(there)

        return send, step

    def weight_line(b, g):
        return line(block(b, g), up_sent.at[b, g], down_sent.at[b, g], line_landed.at[b, g])

    def wide_line(b, g):
        return line(wide(b, g), wide_up_sent.at[b, g], wide_down_sent.at[b, g], wide_line_landed.at[b, g])

    def slim_line(b):
        return line(slim(b, f), slim_up_sent.at[b], slim_down_sent.at[b], slim_line_landed.at[b])

    def walk(make, d, then=None):
        for way in (1, -1):
            b = s - way * d
            inside = (b >= 0) & (b <= n_sp - 1)
            b = jnp.where(inside, b, s)
            make(b)[1](d, b, way, None if then is None else (lambda there, b=b: then(there, b)))

    for copy in own_loads:
        copy.wait()
    weight_line(s, f)[0]()
    for i, p in enumerate(order):
        start(
            remote(decay_piece_ref.at[p], decays_ref.at[f], decay_sent.at[i], decay_landed.at[f], {"fs": p})
        )

    slab = 16

    def spot(owner, core, piece):
        return normed_ref.at[owner, pl.ds(core * half + piece * chunk, chunk), :]

    def normalise(piece):
        @pl.loop(0, chunk // slab)
        def _(i):
            x = raw_ref[pl.ds(piece * chunk + i * slab, slab), :].astype(f32)
            scale = lax.rsqrt(jnp.mean(x * x, axis=-1, keepdims=True) + EPSILON)
            normed_ref[f, pl.ds(t * half + piece * chunk + i * slab, slab), :] = (
                x * scale * gain_ref[...]
            ).astype(bf16)

    def norm_copy(piece, slot, p):
        return remote(
            spot(f, t, piece), spot(f, t, piece), norm_sent.at[slot], norm_landed.at[f, piece], {"fs": p}
        )

    def side_copy(owner, piece):
        view = spot(owner, t, piece)
        return remote(view, view, side_sent.at[owner, piece], side_landed.at[owner, piece], other)

    raw_loads[0].wait()
    normalise(0)
    start(norm_copy(0, 0, xn))
    raw_loads[1].wait()
    normalise(1)
    start(norm_copy(1, 1, yn))
    start(norm_copy(1, 2, xn))
    start(norm_copy(0, 3, yn))
    for piece in range(2):
        start(side_copy(f, piece))

    for p in order:
        remote(pieces_ref.at[p], block(s, p), weight_sent.at[0], weight_landed.at[p], {"fs": p}).wait_recv()
        weight_line(s, p)[0]()
    for copy in out_loads:
        copy.wait()
    for i, p in enumerate(order):
        start(remote(wide(s, f), wide(s, f), wide_sent.at[i], wide_landed.at[f], {"fs": p}))

    for copy in table_loads:
        copy.wait()

    @pl.loop(0, blocks)
    def _(n):
        at = pl.ds(n * BLOCK_LEN, BLOCK_LEN)
        near_cos, near_sin = cos_ref[at, :], sin_ref[at, :]
        cos_ref[at, :] = near_cos * base_ref[0, pl.ds(s, 1), :] - near_sin * base_ref[1, pl.ds(s, 1), :]
        sin_ref[at, :] = near_sin * base_ref[2, pl.ds(s, 1), :] + near_cos * base_ref[3, pl.ds(s, 1), :]

    for p in order:
        remote(
            decay_piece_ref.at[p], decays_ref.at[p], decay_sent.at[0], decay_landed.at[p], {"fs": p}
        ).wait_recv()
    for g in range(n_fs):
        total = decays_ref[g]
        places = lax.broadcasted_iota(jnp.int32, total.shape, 1)
        shift = 1
        while shift < BLOCK_LEN:
            total = total + jnp.where(places >= shift, pltpu.roll(total, shift, 1), 0.0)
            shift *= 2
        decays_ref[g] = total

    def arrived(owner, piece):
        view = spot(owner, t, piece)
        remote(view, view, norm_sent.at[0], norm_landed.at[owner, piece], {"fs": owner}).wait_recv()
        start(side_copy(owner, piece))

    def side_arrived(owner):
        for piece in range(2):
            view = spot(owner, 1 - t, piece)
            remote(view, view, side_sent.at[0, 0], side_landed.at[owner, piece], other).wait_recv()

    def weight_step(d):
        for g in (f,) + order:
            walk(lambda b, g=g: weight_line(b, g), d)

    weight_step(1)
    arrived(xn, 0)
    view = spot(xn, t, 0)
    start(remote(view, view, relay_sent.at[0], norm_landed.at[xn, 0], {"fs": yn}))
    arrived(yn, 1)
    view = spot(yn, t, 1)
    start(remote(view, view, relay_sent.at[1], norm_landed.at[yn, 1], {"fs": xn}))
    for d in range(2, n_sp - 1):
        weight_step(d)
    arrived(xn, 1)
    arrived(yn, 0)

    def slim_plane(b, i):
        return remote(
            slim(b, f), slim(b, f), slim_sent.at[b, i], slim_landed.at[b, f], {"fs": order[i]}
        )

    slim_line(s)[0]()
    for i in range(2):
        start(slim_plane(s, i))
    wide_line(s, f)[0]()
    for p in order:
        remote(wide(s, p), wide(s, p), wide_sent.at[0], wide_landed.at[p], {"fs": p}).wait_recv()
        wide_line(s, p)[0]()

    def slim_spread(there, b):
        for i in range(2):
            start_when(there, slim_plane(b, i))

    def out_step(d):
        walk(slim_line, d, slim_spread)
        for g in (f,) + order:
            walk(lambda b, g=g: wide_line(b, g), d)

    if n_sp > 2:
        weight_step(n_sp - 1)

    def project(o):
        @pl.loop(0, tok // chunk)
        def _(i):
            at = pl.ds(i * chunk, chunk)
            proj_ref[o, at, :] = jnp.dot(
                normed_ref[o, at, :], full_ref[...], preferred_element_type=f32
            ).astype(bf16)

    def part(o, at, index):
        return proj_ref[o, at, lanes + index * VALUE_DIM : lanes + (index + 1) * VALUE_DIM]

    causal = lax.broadcasted_iota(jnp.int32, (BLOCK_LEN, BLOCK_LEN), 0) >= lax.broadcasted_iota(
        jnp.int32, (BLOCK_LEN, BLOCK_LEN), 1
    )
    front = lax.broadcasted_iota(jnp.int32, (BLOCK_LEN, lanes), 1) % KEY_DIM < KEY_DIM // 2

    def retain(o):
        def body(n, carry):
            state, total = carry
            at = pl.ds(pl.multiple_of(n * BLOCK_LEN, BLOCK_LEN), BLOCK_LEN)
            row = decays_ref[o, pl.ds(n, 1), :]
            end = jnp.broadcast_to(row[:, BLOCK_LEN - 1 :], row.shape)
            across = jnp.broadcast_to(row, (BLOCK_LEN, BLOCK_LEN))
            down = across.T
            weighting = jnp.where(causal, jnp.exp(jnp.minimum(down - across, 0.0)), 0.0)
            x = proj_ref[o, at, 0:lanes].astype(f32)
            swapped = jnp.where(
                front, pltpu.roll(x, lanes - KEY_DIM // 2, 1), pltpu.roll(x, KEY_DIM // 2, 1)
            )
            turned = (x * cos_ref[at, :] + swapped * sin_ref[at, :]).astype(bf16)
            queries = turned[:, :KEY_DIM]
            keys = turned.astype(f32).T[KEY_DIM:, :]
            values = part(o, at, 0)
            raw = jnp.dot(queries, keys.astype(bf16), preferred_element_type=f32)
            scores = (raw * weighting).astype(bf16)
            intra_ref[o, at, :] = jnp.dot(scores, values, preferred_element_type=f32)
            decayed_ref[o, at, :] = (queries.astype(f32) * jnp.exp(down[:, :KEY_DIM])).astype(bf16)
            late = (keys * jnp.exp(end - row)).astype(bf16)
            before_ref[o, n] = state
            starts_ref[o, pl.ds(n, 1), :] = total
            product_ref[o, pl.ds(pl.multiple_of(8 + n * BLOCK_LEN, 8), BLOCK_LEN), :] = part(o, at, 3).astype(
                f32
            ) * part(o, at, 4).astype(f32)
            state = state * jnp.exp(end) + jnp.dot(late, values, preferred_element_type=f32)
            return state, total + end

        state, total = lax.fori_loop(
            0, blocks, body, (jnp.zeros((KEY_DIM, VALUE_DIM), f32), jnp.zeros((1, VALUE_DIM), f32))
        )
        state_piece_ref[o] = state.astype(bf16)
        extra_piece_ref[o] = jnp.broadcast_to(total, (8, VALUE_DIM))
        extra_piece_ref[o, 0:halo, :] = product_ref[o, 8 + tok - halo : 8 + tok, :]

    def state_copies(o, owner, d):
        return [
            remote(here, there, state_sent.at[o, d, k], state_landed.at[owner, o, k], {"sp": (s + d) % n_sp})
            for k, (here, there) in enumerate(
                (
                    (state_piece_ref.at[o], states_ref.at[owner, o]),
                    (extra_piece_ref.at[o], extras_ref.at[owner, o]),
                )
            )
        ]

    def pass_state(o):
        for d in range(1, n_sp):
            for copy in state_copies(o, s, d):
                start_when(s + d < n_sp, copy)

    def finish(o, put):
        state_ref[...] = jnp.zeros_like(state_ref)
        product_ref[o, 0:8, :] = jnp.zeros((8, VALUE_DIM), f32)
        for k in range(n_sp - 1):

            @pl.when(k < s)
            def _():
                for copy in state_copies(o, k, 1):
                    copy.wait_recv()
                state_ref[...] = state_ref[...] * jnp.exp(extras_ref[k, o, halo : halo + 1, :]) + states_ref[
                    k, o
                ].astype(f32)

            @pl.when(k == s - 1)
            def _():
                product_ref[o, 8 - halo : 8, :] = extras_ref[k, o, 0:halo, :]

        taps = [taps_ref[k : k + 1, lane(f, VALUE_DIM)] for k in range(CONV_TAPS)]

        @pl.loop(0, blocks)
        def _(n):
            at = pl.ds(pl.multiple_of(n * BLOCK_LEN, BLOCK_LEN), BLOCK_LEN)
            state = before_ref[o, n] + jnp.exp(starts_ref[o, pl.ds(n, 1), :]) * state_ref[...]
            output = intra_ref[o, at, :] + jnp.dot(
                decayed_ref[o, at, :], state.astype(bf16), preferred_element_type=f32
            )
            output = output * lax.rsqrt(jnp.mean(output * output, axis=-1, keepdims=True) + EPSILON)
            gate = part(o, at, 1).astype(f32)
            ret_out = (output * (gate / (1.0 + jnp.exp(-gate)))).astype(bf16)
            padded = product_ref[o, pl.ds(pl.multiple_of(n * BLOCK_LEN, 8), BLOCK_LEN + 8), :]
            convolved = sum(
                taps[k] * padded[8 - halo + k : 8 - halo + k + BLOCK_LEN, :] for k in range(CONV_TAPS)
            )
            conv_out = (part(o, at, 2).astype(f32) * convolved).astype(bf16)
            put(at, ret_out, conv_out)

    def send_mixed(o, i):
        def put(at, ret_out, conv_out):
            mixed_ref[i, at, 0:VALUE_DIM] = ret_out
            mixed_ref[i, at, VALUE_DIM:pair] = conv_out

        finish(o, put)
        start(
            remote(mixed_ref.at[i], merged_ref.at[:, lane(f, pair)], mixed_sent.at[i], mixed_landed.at[f], {"fs": o})
        )

    def keep(at, ret_out, conv_out):
        merged_ref[at, lane(2 * f, VALUE_DIM)] = ret_out
        merged_ref[at, lane(2 * f + 1, VALUE_DIM)] = conv_out

    def local_stage(o):
        side_arrived(o)
        project(o)
        retain(o)
        pass_state(o)

    local_stage(xn)
    local_stage(yn)
    send_mixed(xn, 0)
    arrived(dn, 0)
    arrived(dn, 1)
    local_stage(dn)
    send_mixed(yn, 1)
    out_step(1)

    def slim_arrived(b, g):
        remote(
            slim(b, g), slim(b, g), slim_relay_sent.at[0], slim_landed.at[b, g], {"fs": g}
        ).wait_recv()

    def slim_relay(b, first, onward):
        slim_arrived(b, first)
        start(
            remote(slim(b, first), slim(b, first), slim_relay_sent.at[b], slim_landed.at[b, first], {"fs": onward})
        )

    local_stage(f)
    send_mixed(dn, 2)
    for d in range(2, n_sp - 1):
        out_step(d)
    finish(f, keep)
    if n_sp > 2:
        out_step(n_sp - 1)
    for b in range(n_sp):
        first, onward = (xn, yn) if b < n_sp // 2 else (yn, xn)
        slim_relay(b, first, onward)
    for p in order:
        view = merged_ref.at[:, lane(p, pair)]
        remote(view, view, mixed_sent.at[0], mixed_landed.at[p], {"fs": p}).wait_recv()
    for b in range(n_sp):
        slim_arrived(b, yn if b < n_sp // 2 else xn)
        slim_arrived(b, dn)

    tiles = part_ref.shape[0]
    tile = part_ref.shape[2]

    def partial_tile(core, i):
        return lax.dot_general(
            merged_ref[pl.ds(core * half, half), :],
            outs_ref[pl.ds(pl.multiple_of(i * tile, tile), tile), :],
            (((1,), (1,)), ((), ())),
            preferred_element_type=f32,
        ).astype(bf16)

    def part_copy(i):
        return remote(part_ref.at[i], far_ref.at[i], part_sent.at[i], part_landed.at[i], other)

    @pl.loop(0, tiles)
    def _(i):
        part_ref[i] = partial_tile(1 - t, i)
        part_copy(i).start()

    @pl.loop(0, tiles)
    def _(i):
        mine = partial_tile(t, i).astype(f32)
        part_copy(i).wait_recv()
        out_ref[:, lane(i, tile)] = (mine + far_ref[i].astype(f32)).astype(bf16)

    @pl.loop(0, tiles)
    def _(i):
        part_copy(i).wait_send()

    for copy in waits:
        copy.wait_send()
    for condition, copy in guarded:

        @pl.when(condition)
        def _():
            copy.wait_send()


def fast_shards(
    tokens,
    norm_gain,
    query_weight,
    key_weight,
    value_weight,
    gate_weight,
    conv_b_weight,
    conv_c_weight,
    conv_in_weight,
    conv_kernel,
    out_ret_weight,
    out_conv_weight,
    log_decay,
):
    n_sp, n_fs = lax.axis_size("sp"), lax.axis_size("fs")
    tok, model = tokens.shape[1:]
    half = tok // 2
    blocks = tok // BLOCK_LEN
    rows = query_weight.shape[0]
    width = 2 * KEY_DIM + 5 * VALUE_DIM
    lanes, pair = 2 * KEY_DIM, 2 * VALUE_DIM
    tile = min(OUT_TILE, model)

    frequency = np.tile(1.0 / ROPE_BASE ** np.linspace(0.0, 1.0, KEY_DIM // 2), 4)
    near = np.arange(tok)[:, None] * frequency[None, :]
    far = (np.arange(n_sp) * tok)[:, None] * frequency[None, :]
    scale = np.where(np.arange(lanes) < KEY_DIM, 1.0, KEY_DIM ** (-0.5))
    sign = np.where(np.arange(lanes) % KEY_DIM < KEY_DIM // 2, -1.0, 1.0)
    base = np.stack(
        [np.cos(far) * scale, np.sin(far) * scale, np.cos(far) * scale * sign, np.sin(far) * scale * sign]
    )

    any_space = pl.BlockSpec(memory_space=pl.ANY)
    vmem = pl.BlockSpec(memory_space=pltpu.VMEM)
    dma = pltpu.SemaphoreType.DMA
    f32, bf16 = jnp.float32, jnp.bfloat16
    buffers = [
        ((half, model), bf16),
        ((n_fs, tok, model), bf16),
        ((n_fs, rows, width), bf16),
        ((2, rows, n_fs * KEY_DIM), bf16),
        ((n_sp * n_fs * rows, width), bf16),
        ((n_sp * n_fs * rows, n_fs * pair), bf16),
        ((n_fs, 8, BLOCK_LEN), f32),
        ((n_fs, 8, BLOCK_LEN), f32),
        ((tok, lanes), f32),
        ((tok, lanes), f32),
        ((n_fs, tok, width), bf16),
        ((n_fs, tok, VALUE_DIM), f32),
        ((n_fs, tok, KEY_DIM), bf16),
        ((n_fs, blocks, KEY_DIM, VALUE_DIM), f32),
        ((n_fs, 8, VALUE_DIM), f32),
        ((n_fs, 8 + tok, VALUE_DIM), f32),
        ((KEY_DIM, VALUE_DIM), f32),
        ((n_fs, KEY_DIM, VALUE_DIM), bf16),
        ((n_sp, n_fs, KEY_DIM, VALUE_DIM), bf16),
        ((n_fs, 8, VALUE_DIM), f32),
        ((n_sp, n_fs, 8, VALUE_DIM), f32),
        ((n_fs - 1, tok, pair), bf16),
        ((tok, n_fs * pair), bf16),
        ((model // tile, half, tile), bf16),
        ((model // tile, half, tile), bf16),
    ]
    semaphores = [
        (48,),
        (3,),
        (n_fs,),
        (3,),
        (n_fs,),
        (4,),
        (n_fs, 2),
        (n_fs, 2),
        (n_fs, 2),
        (2,),
        (n_sp, n_fs),
        (n_sp, n_fs),
        (n_sp, n_fs),
        (3,),
        (n_fs,),
        (n_sp, n_fs),
        (n_sp, n_fs),
        (n_sp, n_fs),
        (n_sp,),
        (n_sp,),
        (n_sp,),
        (n_sp, 2),
        (n_sp, n_fs),
        (n_sp,),
        (n_fs, n_sp, 2),
        (n_sp, n_fs, 2),
        (n_fs - 1,),
        (n_fs,),
        (model // tile,),
        (model // tile,),
    ]
    mixed = pl.pallas_call(
        lambda *refs: mixer_kernel(n_sp, *refs),
        out_shape=jax.ShapeDtypeStruct((half, model), bf16),
        in_specs=[any_space, vmem] + [any_space] * 7 + [vmem] + [any_space] * 2 + [vmem] + [any_space] * 2 + [vmem],
        out_specs=vmem,
        scratch_shapes=[pltpu.VMEM(shape, kind) for shape, kind in buffers] + [dma(shape) for shape in semaphores],
        compiler_params=pltpu.CompilerParams(
            collective_id=0, has_side_effects=True, vmem_limit_bytes=60 * 1024 * 1024
        ),
        name="mixer",
    )(
        tokens,
        norm_gain.reshape(1, model),
        query_weight,
        key_weight,
        value_weight,
        gate_weight,
        conv_b_weight,
        conv_c_weight,
        conv_in_weight,
        conv_kernel,
        out_ret_weight,
        out_conv_weight,
        log_decay,
        jnp.asarray(np.cos(near), jnp.float32),
        jnp.asarray(np.sin(near), jnp.float32),
        jnp.asarray(base, jnp.float32),
    )
    return mixed[None]


def select(mesh):
    def chosen(*arrays):
        heads, conv_width = arrays[12].shape[1], arrays[9].shape[1]
        n_sp, n_fs, n_tp = (mesh.shape[name] for name in ("sp", "fs", "tp"))
        tok, model = arrays[0].shape[1:]
        fits = n_fs == 4 and n_tp == 2 and n_sp > 2 and heads == n_fs
        fits = fits and conv_width == n_fs * VALUE_DIM and tok % (2 * BLOCK_LEN) == 0
        fits = fits and tok // BLOCK_LEN <= 8 and model % OUT_TILE == 0
        return (fast_shards if fits else shards)(*arrays)

    return chosen


def solution(mesh):
    in_specs = (
        P("fs", "sp", None),
        P(),
        P(("sp", "fs"), "tp"),
        P(("sp", "fs"), "tp"),
        P(("sp", "fs"), "tp"),
        P(("sp", "fs"), "tp"),
        P(("sp", "fs"), "tp"),
        P(("sp", "fs"), "tp"),
        P(("sp", "fs"), "tp"),
        P(None, "tp"),
        P(("sp", "fs"), "tp"),
        P(("sp", "fs"), "tp"),
        P("fs", "tp", "sp"),
    )
    out_specs = P("fs", ("sp", "tp"), None)
    return jax.shard_map(select(mesh), mesh=mesh, in_specs=in_specs, out_specs=out_specs, check_vma=False)
```

time: 207 us -> 131 us (0.63)
  other arithmetic: 30.5 us -> 0 us
  matrix products: 19.5 us -> 0 us
  local copies, waits for them, and re-layouts: 17 us -> 2.73 us
  Pallas kernels: 138 us -> 127 us
    dot_general x5 -> x0, matrix products: 19.5 us -> none  [the longest x2 12 us: project(): lax.dot_general(spread(piece), weight, (((1,), (1,)), ((), ())), preferre...]
    pallas_call x3 -> x1, Pallas kernels: 138 us -> 127 us  [fast_shards(): pl.pallas_call(lambda *refs: mixer_kernel(n_sp, *refs), out_shape=jax.Sha...]
    another operation x4 -> x0, other arithmetic: 8.8 us -> none
    convert_element_type x4 -> x0, other arithmetic: 6.51 us -> none  [the longest x1 3.05 us: fast_shards(): normed = (inputs * lax.rsqrt(jnp.mean(inputs * inputs, axis=-1, keepdims=...]
    concatenate x5 -> x0, local copies, waits for them, and re-layouts: 6.16 us -> none  [the longest x4 5 us: rotate_flat(): jnp.concatenate([first * cosine - second * sine, first * sine + second *...]
    reshape x11 -> x0, local copies, waits for them, and re-layouts: 4.56 us -> none  [the longest x4 3.61 us: spread(): parts = piece.reshape(n_fs, half, 2, width)]
    mul x2 -> x0, other arithmetic: 3.48 us -> none  [the longest x1 1.88 us: fast_shards(): output * lax.rsqrt(jnp.mean(output * output, axis=-1, keepdims=True) + EP...]
    concatenate x3 -> x0, other arithmetic: 2.67 us -> none  [the longest x1 1.32 us: fast_shards(): jnp.concatenate([ret_out, conv_out], axis=-1)]
where the time goes in v1:
time: 131 us; the launch traced here: 130 us
  Pallas kernels  127 us (97%)
  local copies, waits for them, and re-layouts  2.73 us (2%)
    pallas_call x1, Pallas kernels, fast_shards(): pl.pallas_call(lambda *refs: mixer_kernel(n_sp, *refs), out_shape=jax.Sha...  127 us
    unnamed x1, local copies, waits for them, and re-layouts  2.73 us

profile of v1, /device:TPU:0, one launch (start us, length us, event | category | flops | bytes accessed | tf_op | source)
XLA Modules:
  0.0 130.0 jit_solution(316368426093206530)
XLA Ops:
  0.0 127.2 %mixer.1 = bf16[384,2048]{1,0:T(8,128)(2,1)} custom-call(bf16[1,768,2048]{2,1,0:T(8,128)(2,1)} %refs_0_.1, f32[1,2048]{1,0:T(1,128)} %bitcast.3, bf16[128,256]{1,0:T(8,128)(2,1)} %refs_2_.1, bf16[128,256]{1,0:T(8,128)(2,1)} %refs_3_.1, bf16[128,512]{1,0:T(8,128)(2,1)} %refs_4_.1, bf16[128,512]{1,0:T(8,128)(2,1)} %refs_5_.1, bf16[128,512]{1,0:T(8,128)(2,1)} %refs_6_.1, ...), custom_call_target="tpu_custom_call" | custom-call | tf_op jit(solution)/shard_map/mixer/pallas_call | solution.py:889
  127.3 2.7 %copy.18 = bf16[1,384,2048]{2,1,0:T(8,128)(2,1)} copy(bf16[1,384,2048]{2,1,0:T(8,128)(2,1)} %bitcast.2) | data formatting | bytes 3145728

commit v2 on v1

--- a/solution.py
+++ b/solution.py
@@ -220,8 +220,7 @@
 
 
 MESH_IDS = pl.DeviceIdType.MESH
-OUT_CUT = 2
-OUT_TILE = 512
+WIDE_SHARE = 4
 
 
 def remote(source, target, sent, landed, device):
@@ -276,6 +275,7 @@
     decays_ref,
     cos_ref,
     sin_ref,
+    early_ref,
     proj_ref,
     intra_ref,
     decayed_ref,
@@ -283,46 +283,26 @@
     starts_ref,
     product_ref,
     state_ref,
+    extra_ref,
     state_piece_ref,
     states_ref,
-    extra_piece_ref,
-    extras_ref,
     mixed_ref,
     merged_ref,
     part_ref,
     far_ref,
     local_sem,
-    weight_sent,
-    weight_landed,
-    decay_sent,
-    decay_landed,
-    norm_sent,
+    send_sem,
+    full_landed,
+    wide_landed,
+    slim_landed,
     norm_landed,
-    side_sent,
     side_landed,
-    relay_sent,
-    up_sent,
-    down_sent,
-    line_landed,
-    wide_sent,
-    wide_landed,
-    wide_up_sent,
-    wide_down_sent,
-    wide_line_landed,
-    slim_up_sent,
-    slim_down_sent,
-    slim_line_landed,
-    slim_sent,
-    slim_landed,
-    slim_relay_sent,
-    state_sent,
     state_landed,
-    mixed_sent,
-    mixed_landed,
-    part_sent,
     part_landed,
+    once_landed,
 ):
     f32, bf16 = jnp.float32, jnp.bfloat16
+    scope = jax.named_scope
     s, f, t = lax.axis_index("sp"), lax.axis_index("fs"), lax.axis_index("tp")
     xn, yn, dn = plane_partners(f)
     order = (xn, yn, dn)
@@ -331,148 +311,158 @@
     half = tok // 2
     chunk = half // 2
     rows = query_ref.shape[0]
+    slab_rows = n_fs * rows
     blocks = tok // BLOCK_LEN
     lanes = 2 * KEY_DIM
     pair = 2 * VALUE_DIM
     halo = CONV_TAPS - 1
-    cut = rows // OUT_CUT
+    cut = rows * WIDE_SHARE // 8
 
     def lane(index, width):
         return pl.ds(pl.multiple_of(index * width, width), width)
 
-    waits = []
-    guarded = []
-
-    def start(copy):
-        copy.start()
-        waits.append(copy)
-
-    def start_when(condition, copy):
-        @pl.when(condition)
-        def _():
-            copy.start()
-
-        guarded.append((condition, copy))
-
-    count = [0]
-
-    def fetch(source, target):
-        copy = pltpu.make_async_copy(source, target, local_sem.at[count[0]])
-        count[0] += 1
+    names = (
+        "weight", "decay", "norm", "side", "relay", "up", "down", "wide", "wide_relay", "wide_up", "wide_down",
+        "slim", "slim_relay", "slim_up", "slim_down", "state", "mixed", "part",
+    )
+    sent = {name: send_sem.at[i] for i, name in enumerate(names)}
+
+    def all_sent(name, view):
+        remote(view, view, sent[name], once_landed.at[0], other).wait_send()
+
+    def line_sent(name, view_of):
+        for i in range(n_sp - 1):
+            here = i if name.endswith("up") else n_sp - 1 - i
+
+            @pl.when(s == here)
+            def _(i=i):
+                all_sent(name, view_of(i + 1))
+
+    def fetch(source, target, slot):
+        copy = pltpu.make_async_copy(source, target, local_sem.at[slot])
         copy.start()
         return copy
 
+    def fetched(view, slot):
+        pltpu.make_async_copy(view, view, local_sem.at[slot]).wait()
+
+    def own_rows(b, g):
+        return pl.ds((b * n_fs + g) * rows, rows)
+
     def block(b, g):
-        return full_ref.at[pl.ds((b * n_fs + g) * rows, rows), :]
+        return full_ref.at[own_rows(b, g), :]
 
     def wide(b, g):
         return outs_ref.at[pl.ds((b * n_fs + g) * rows, cut), :]
 
+    def wide_half(g, i):
+        width = outs_ref.shape[1] // 2
+        return outs_ref.at[pl.ds((s * n_fs + g) * rows, cut), pl.ds(i * width, width)]
+
     def slim(b, g):
         return outs_ref.at[pl.ds((b * n_fs + g) * rows + cut, rows - cut), :]
 
-    head_loads = [fetch(query_ref, heads_ref.at[0]), fetch(key_ref, heads_ref.at[1])]
+    fetch(query_ref, heads_ref.at[0], 0)
+    fetch(key_ref, heads_ref.at[1], 0)
     wide_weights = (value_ref, gate_ref, conv_b_ref, conv_c_ref, conv_in_ref)
-    piece_loads = []
     for p in range(n_fs):
         for j, weight in enumerate(wide_weights):
-            piece_loads.append(
-                fetch(
-                    weight.at[:, pl.ds(p * VALUE_DIM, VALUE_DIM)],
-                    pieces_ref.at[p, :, pl.ds(lanes + j * VALUE_DIM, VALUE_DIM)],
-                )
+            fetch(
+                weight.at[:, pl.ds(p * VALUE_DIM, VALUE_DIM)],
+                pieces_ref.at[p, :, pl.ds(lanes + j * VALUE_DIM, VALUE_DIM)],
+                1,
             )
-    own_loads = [
+    for j, weight in enumerate(wide_weights):
         fetch(
             weight.at[:, lane(f, VALUE_DIM)],
-            full_ref.at[pl.ds((s * n_fs + f) * rows, rows), pl.ds(lanes + j * VALUE_DIM, VALUE_DIM)],
+            full_ref.at[own_rows(s, f), pl.ds(lanes + j * VALUE_DIM, VALUE_DIM)],
+            2,
         )
-        for j, weight in enumerate(wide_weights)
-    ]
-    raw_loads = [
+    for i in range(2):
         fetch(
-            tokens_ref.at[0, pl.ds(t * half + i * chunk, chunk), :], raw_ref.at[pl.ds(i * chunk, chunk), :]
+            tokens_ref.at[0, pl.ds(t * half + i * chunk, chunk), :],
+            raw_ref.at[pl.ds(i * chunk, chunk), :],
+            3 + i,
         )
-        for i in range(2)
-    ]
-    out_loads = []
     for g in range(n_fs):
         for j, weight in enumerate((out_ret_ref, out_conv_ref)):
-            out_loads.append(
-                fetch(
-                    weight.at[:, pl.ds(g * VALUE_DIM, VALUE_DIM)],
-                    outs_ref.at[
-                        pl.ds((s * n_fs + f) * rows, rows), pl.ds(g * pair + j * VALUE_DIM, VALUE_DIM)
-                    ],
-                )
+            fetch(
+                weight.at[:, pl.ds(g * VALUE_DIM, VALUE_DIM)],
+                outs_ref.at[own_rows(s, f), pl.ds(g * pair + j * VALUE_DIM, VALUE_DIM)],
+                5,
             )
-    table_loads = [fetch(near_cos_ref, cos_ref), fetch(near_sin_ref, sin_ref)]
-
-    peers = [{"fs": p} for p in order] + [other]
-    peers += [{"sp": (s + d) % n_sp} for d in range(1, n_sp)]
-    greet(peers)
-
-    for copy in head_loads:
-        copy.wait()
+    tables = [fetch(near_cos_ref, cos_ref, 6), fetch(near_sin_ref, sin_ref, 7)]
+
+    with scope("greet"):
+        peers = [{"fs": p} for p in order] + [other]
+        peers += [{"sp": (s + d) % n_sp} for d in range(1, n_sp)]
+        greet(peers)
+
+    fetched(heads_ref, 0)
     for p in range(n_fs):
         own = pl.ds(p * KEY_DIM, KEY_DIM)
         pieces_ref[p, :, 0:lanes] = jnp.concatenate([heads_ref[0, :, own], heads_ref[1, :, own]], axis=-1)
-    full_ref[pl.ds((s * n_fs + f) * rows, rows), 0:lanes] = pieces_ref[f, :, 0:lanes]
+    full_ref[own_rows(s, f), 0:lanes] = pieces_ref[f, :, 0:lanes]
     decay_piece_ref[...] = jnp.zeros_like(decay_piece_ref)
     for p in range(n_fs):
         for n in range(blocks):
             decay_piece_ref[p, n : n + 1, :] = decay_ref[0, p : p + 1, n * BLOCK_LEN : (n + 1) * BLOCK_LEN]
     decays_ref[f] = decay_piece_ref[f]
-    for copy in piece_loads:
-        copy.wait()
-    for i, p in enumerate(order):
-        start(remote(pieces_ref.at[p], block(s, f), weight_sent.at[i], weight_landed.at[f], {"fs": p}))
+    fetched(pieces_ref.at[:, :, lanes:], 1)
+    for p in order:
+        remote(pieces_ref.at[p], block(s, f), sent["weight"], full_landed.at[s, f], {"fs": p}).start()
 
     def line(view, up, down, landed):
-        def copy(source, way):
-            return remote(source, view, up if way == 1 else down, landed, {"sp": s + way})
+        def copy(way):
+            return remote(view, view, sent[up] if way == 1 else sent[down], landed, {"sp": s + way})
 
         def send():
-            start_when(s < n_sp - 1, copy(view, 1))
-            start_when(s > 0, copy(view, -1))
-
-        def step(d, b, way, then):
-            there = (s - d >= 0) if way == 1 else (s + d <= n_sp - 1)
-            further = there & ((s < n_sp - 1) if way == 1 else (s > 0))
+            @pl.when(s < n_sp - 1)
+            def _():
+                copy(1).start()
+
+            @pl.when(s > 0)
+            def _():
+                copy(-1).start()
+
+        def step(way, there, then):
+            further = (s < n_sp - 1) if way == 1 else (s > 0)
 
             @pl.when(there)
             def _():
-                copy(view, way).wait_recv()
-
-            start_when(further, copy(view, way))
-            if then is not None:
-                then(there)
+                copy(way).wait_recv()
+
+                @pl.when(further)
+                def _():
+                    copy(way).start()
+
+                if then is not None:
+                    then()
 
         return send, step
 
     def weight_line(b, g):
-        return line(block(b, g), up_sent.at[b, g], down_sent.at[b, g], line_landed.at[b, g])
+        return line(block(b, g), "up", "down", full_landed.at[b, g])
 
     def wide_line(b, g):
-        return line(wide(b, g), wide_up_sent.at[b, g], wide_down_sent.at[b, g], wide_line_landed.at[b, g])
+        return line(wide(b, g), "wide_up", "wide_down", wide_landed.at[b, g])
 
     def slim_line(b):
-        return line(slim(b, f), slim_up_sent.at[b], slim_down_sent.at[b], slim_line_landed.at[b])
+        return line(slim(b, f), "slim_up", "slim_down", slim_landed.at[b, f])
 
     def walk(make, d, then=None):
         for way in (1, -1):
             b = s - way * d
-            inside = (b >= 0) & (b <= n_sp - 1)
-            b = jnp.where(inside, b, s)
-            make(b)[1](d, b, way, None if then is None else (lambda there, b=b: then(there, b)))
-
-    for copy in own_loads:
-        copy.wait()
+            there = (b >= 0) & (b <= n_sp - 1)
+            b = jnp.where(there, b, s)
+            make(b)[1](way, there, None if then is None else (lambda b=b: then(b)))
+
+    fetched(full_ref.at[own_rows(s, f), lanes:], 2)
     weight_line(s, f)[0]()
-    for i, p in enumerate(order):
-        start(
-            remote(decay_piece_ref.at[p], decays_ref.at[f], decay_sent.at[i], decay_landed.at[f], {"fs": p})
-        )
+    for p in order:
+        remote(
+            decay_piece_ref.at[p], decays_ref.at[f], sent["decay"], once_landed.at[1], {"fs": p}
+        ).start()
 
     slab = 16
 
@@ -488,35 +478,35 @@
                 x * scale * gain_ref[...]
             ).astype(bf16)
 
-    def norm_copy(piece, slot, p):
-        return remote(
-            spot(f, t, piece), spot(f, t, piece), norm_sent.at[slot], norm_landed.at[f, piece], {"fs": p}
-        )
+    def norm_copy(owner, piece, kind, p):
+        view = spot(owner, t, piece)
+        return remote(view, view, sent[kind], norm_landed.at[owner, piece], {"fs": p})
 
     def side_copy(owner, piece):
         view = spot(owner, t, piece)
-        return remote(view, view, side_sent.at[owner, piece], side_landed.at[owner, piece], other)
-
-    raw_loads[0].wait()
-    normalise(0)
-    start(norm_copy(0, 0, xn))
-    raw_loads[1].wait()
-    normalise(1)
-    start(norm_copy(1, 1, yn))
-    start(norm_copy(1, 2, xn))
-    start(norm_copy(0, 3, yn))
-    for piece in range(2):
-        start(side_copy(f, piece))
-
-    for p in order:
-        remote(pieces_ref.at[p], block(s, p), weight_sent.at[0], weight_landed.at[p], {"fs": p}).wait_recv()
-        weight_line(s, p)[0]()
-    for copy in out_loads:
-        copy.wait()
-    for i, p in enumerate(order):
-        start(remote(wide(s, f), wide(s, f), wide_sent.at[i], wide_landed.at[f], {"fs": p}))
-
-    for copy in table_loads:
+        remote(view, view, sent["side"], side_landed.at[owner], other).start()
+
+    with scope("norm"):
+        fetched(raw_ref.at[0:chunk, :], 3)
+        normalise(0)
+        norm_copy(f, 0, "norm", xn).start()
+        fetched(raw_ref.at[chunk:half, :], 4)
+        normalise(1)
+        norm_copy(f, 1, "norm", yn).start()
+        norm_copy(f, 1, "norm", xn).start()
+        norm_copy(f, 0, "norm", yn).start()
+        for piece in range(2):
+            side_copy(f, piece)
+
+    with scope("w_plane"):
+        for p in order:
+            remote(pieces_ref.at[p], block(s, p), sent["weight"], full_landed.at[s, p], {"fs": p}).wait_recv()
+            weight_line(s, p)[0]()
+    fetched(outs_ref.at[own_rows(s, f), :], 5)
+    for p in order[:2]:
+        remote(wide(s, f), wide(s, f), sent["wide"], wide_landed.at[s, f], {"fs": p}).start()
+
+    for copy in tables:
         copy.wait()
 
     @pl.loop(0, blocks)
@@ -526,10 +516,8 @@
         cos_ref[at, :] = near_cos * base_ref[0, pl.ds(s, 1), :] - near_sin * base_ref[1, pl.ds(s, 1), :]
         sin_ref[at, :] = near_sin * base_ref[2, pl.ds(s, 1), :] + near_cos * base_ref[3, pl.ds(s, 1), :]
 
-    for p in order:
-        remote(
-            decay_piece_ref.at[p], decays_ref.at[p], decay_sent.at[0], decay_landed.at[p], {"fs": p}
-        ).wait_recv()
+    view = decay_piece_ref.at[0 : len(order)]
+    remote(view, view, sent["decay"], once_landed.at[1], other).wait_recv()
     for g in range(n_fs):
         total = decays_ref[g]
         places = lax.broadcasted_iota(jnp.int32, total.shape, 1)
@@ -540,63 +528,129 @@
         decays_ref[g] = total
 
     def arrived(owner, piece):
-        view = spot(owner, t, piece)
-        remote(view, view, norm_sent.at[0], norm_landed.at[owner, piece], {"fs": owner}).wait_recv()
-        start(side_copy(owner, piece))
+        norm_copy(owner, piece, "norm", owner).wait_recv()
+        side_copy(owner, piece)
 
     def side_arrived(owner):
-        for piece in range(2):
-            view = spot(owner, 1 - t, piece)
-            remote(view, view, side_sent.at[0, 0], side_landed.at[owner, piece], other).wait_recv()
+        with scope("side"):
+            view = normed_ref.at[owner, pl.ds((1 - t) * half, half), :]
+            remote(view, view, sent["side"], side_landed.at[owner], other).wait_recv()
 
     def weight_step(d):
-        for g in (f,) + order:
-            walk(lambda b, g=g: weight_line(b, g), d)
+        with scope(f"w_line#d={d}"):
+            for g in (f,) + order:
+                walk(lambda b, g=g: weight_line(b, g), d)
+
+    def nearest(k):
+        ranked = [sorted(range(n_sp), key=lambda b: (abs(b - here), b))[k] for here in range(n_sp)]
+        return sum(jnp.where(s == here, b, 0) for here, b in enumerate(ranked))
+
+    def columns(o, at, b):
+        return jnp.dot(
+            normed_ref[o, at, lane(b, slab_rows)],
+            full_ref[pl.ds(pl.multiple_of(b * slab_rows, slab_rows), slab_rows), :],
+            preferred_element_type=f32,
+        )
+
+    def project_early(o, i):
+        side_arrived(o)
+        with scope("early"):
+            near = [nearest(k) for k in range(n_sp - 1)]
+
+            @pl.loop(0, tok // chunk)
+            def _(j):
+                at = pl.ds(j * chunk, chunk)
+                early_ref[i, at, :] = sum(columns(o, at, b) for b in near)
+
+    def project_late(o, i):
+        with scope("late"):
+            last = nearest(n_sp - 1)
+
+            @pl.loop(0, tok // chunk)
+            def _(j):
+                at = pl.ds(j * chunk, chunk)
+                proj_ref[o, at, :] = (early_ref[i, at, :] + columns(o, at, last)).astype(bf16)
+
+    def project(o):
+        side_arrived(o)
+        with scope("project"):
+
+            @pl.loop(0, tok // chunk)
+            def _(j):
+                at = pl.ds(j * chunk, chunk)
+                proj_ref[o, at, :] = jnp.dot(
+                    normed_ref[o, at, :], full_ref[...], preferred_element_type=f32
+                ).astype(bf16)
 
     weight_step(1)
-    arrived(xn, 0)
-    view = spot(xn, t, 0)
-    start(remote(view, view, relay_sent.at[0], norm_landed.at[xn, 0], {"fs": yn}))
-    arrived(yn, 1)
-    view = spot(yn, t, 1)
-    start(remote(view, view, relay_sent.at[1], norm_landed.at[yn, 1], {"fs": xn}))
+    with scope("x_first"):
+        arrived(xn, 0)
+        norm_copy(xn, 0, "relay", yn).start()
+        arrived(yn, 1)
+        norm_copy(yn, 1, "relay", xn).start()
     for d in range(2, n_sp - 1):
         weight_step(d)
-    arrived(xn, 1)
-    arrived(yn, 0)
-
-    def slim_plane(b, i):
-        return remote(
-            slim(b, f), slim(b, f), slim_sent.at[b, i], slim_landed.at[b, f], {"fs": order[i]}
-        )
-
     slim_line(s)[0]()
-    for i in range(2):
-        start(slim_plane(s, i))
     wide_line(s, f)[0]()
-    for p in order:
-        remote(wide(s, p), wide(s, p), wide_sent.at[0], wide_landed.at[p], {"fs": p}).wait_recv()
-        wide_line(s, p)[0]()
-
-    def slim_spread(there, b):
-        for i in range(2):
-            start_when(there, slim_plane(b, i))
-
-    def out_step(d):
-        walk(slim_line, d, slim_spread)
-        for g in (f,) + order:
-            walk(lambda b, g=g: wide_line(b, g), d)
-
-    if n_sp > 2:
-        weight_step(n_sp - 1)
-
-    def project(o):
-        @pl.loop(0, tok // chunk)
-        def _(i):
-            at = pl.ds(i * chunk, chunk)
-            proj_ref[o, at, :] = jnp.dot(
-                normed_ref[o, at, :], full_ref[...], preferred_element_type=f32
-            ).astype(bf16)
+    project_early(f, 0)
+    with scope("x_second"):
+        arrived(xn, 1)
+        arrived(yn, 0)
+
+    with scope("wide_plane"):
+        for i, p in enumerate(order[:2]):
+            remote(wide(s, p), wide(s, p), sent["wide"], wide_landed.at[s, p], {"fs": p}).wait_recv()
+            view = wide_half(p, i)
+            remote(view, view, sent["wide_relay"], wide_landed.at[s, p], {"fs": order[1 - i]}).start()
+
+    def wide_far():
+        with scope("wide_far"):
+            remote(wide(s, dn), wide(s, dn), sent["wide"], wide_landed.at[s, dn], {"fs": dn}).wait_recv()
+
+    def slim_spread(b):
+        for p in order[:2]:
+            remote(slim(b, f), slim(b, f), sent["slim"], slim_landed.at[b, f], {"fs": p}).start()
+
+    def slim_arrived(b, g):
+        remote(slim(b, g), slim(b, g), sent["slim"], slim_landed.at[b, g], {"fs": g}).wait_recv()
+
+    def at_distance(d):
+        for way in (1, -1) if d else (1,):
+            b = s - way * d
+            there = (b >= 0) & (b <= n_sp - 1)
+            yield jnp.where(there, b, s), there
+
+    def slim_plane(d):
+        for b, there in at_distance(d):
+            pl.when(there)(lambda b=b: slim_spread(b))
+
+    def slim_relay(d):
+        with scope(f"relay#d={d}"):
+            for b, there in at_distance(d):
+                near = b < n_sp // 2
+                first, onward = jnp.where(near, xn, yn), jnp.where(near, yn, xn)
+
+                @pl.when(there)
+                def _():
+                    slim_arrived(b, first)
+                    view = slim(b, first)
+                    remote(view, view, sent["slim_relay"], slim_landed.at[b, first], {"fs": onward}).start()
+
+    def slim_rest(d):
+        for b, there in at_distance(d):
+
+            @pl.when(there)
+            def _():
+                slim_arrived(b, jnp.where(b < n_sp // 2, yn, xn))
+                slim_arrived(b, dn)
+
+    def slim_step(d):
+        with scope(f"slim#d={d}"):
+            walk(slim_line, d)
+
+    def wide_step(d, g):
+        with scope(f"wide#d={d}"):
+            walk(lambda b: wide_line(b, g), d)
 
     def part(o, at, index):
         return proj_ref[o, at, lanes + index * VALUE_DIM : lanes + (index + 1) * VALUE_DIM]
@@ -605,6 +659,9 @@
         jnp.int32, (BLOCK_LEN, BLOCK_LEN), 1
     )
     front = lax.broadcasted_iota(jnp.int32, (BLOCK_LEN, lanes), 1) % KEY_DIM < KEY_DIM // 2
+
+    def rounded(x):
+        return x.astype(bf16).astype(f32)
 
     def retain(o):
         def body(n, carry):
@@ -636,158 +693,194 @@
             state = state * jnp.exp(end) + jnp.dot(late, values, preferred_element_type=f32)
             return state, total + end
 
-        state, total = lax.fori_loop(
-            0, blocks, body, (jnp.zeros((KEY_DIM, VALUE_DIM), f32), jnp.zeros((1, VALUE_DIM), f32))
+        with scope("retain"):
+            state, total = lax.fori_loop(
+                0, blocks, body, (jnp.zeros((KEY_DIM, VALUE_DIM), f32), jnp.zeros((1, VALUE_DIM), f32))
+            )
+            rim = product_ref[o, 8 + tok - halo : 8 + tok, :]
+            middle = total - rounded(total)
+            extra_ref[...] = jnp.zeros_like(extra_ref)
+            extra_ref[0:halo, :] = rounded(rim)
+            extra_ref[halo : 2 * halo, :] = rim - rounded(rim)
+            extra_ref[8:9, :] = rounded(total)
+            extra_ref[9:10, :] = rounded(middle)
+            extra_ref[10:11, :] = middle - rounded(middle)
+            state_piece_ref[o, 0:KEY_DIM, :] = state.astype(bf16)
+            state_piece_ref[o, KEY_DIM:, :] = extra_ref[...].astype(bf16)
+            for d in range(1, n_sp):
+
+                @pl.when(s + d < n_sp)
+                def _():
+                    state_copy(o, s, d).start()
+
+    def state_copy(o, owner, d):
+        return remote(
+            state_piece_ref.at[o],
+            states_ref.at[owner, o],
+            sent["state"],
+            state_landed.at[owner, o],
+            {"sp": (s + d) % n_sp},
         )
-        state_piece_ref[o] = state.astype(bf16)
-        extra_piece_ref[o] = jnp.broadcast_to(total, (8, VALUE_DIM))
-        extra_piece_ref[o, 0:halo, :] = product_ref[o, 8 + tok - halo : 8 + tok, :]
-
-    def state_copies(o, owner, d):
-        return [
-            remote(here, there, state_sent.at[o, d, k], state_landed.at[owner, o, k], {"sp": (s + d) % n_sp})
-            for k, (here, there) in enumerate(
-                (
-                    (state_piece_ref.at[o], states_ref.at[owner, o]),
-                    (extra_piece_ref.at[o], extras_ref.at[owner, o]),
+
+    def finish(o, put):
+        with scope("state"):
+            state_ref[...] = jnp.zeros_like(state_ref)
+            product_ref[o, 0:8, :] = jnp.zeros((8, VALUE_DIM), f32)
+            for k in range(n_sp - 1):
+
+                @pl.when(k < s)
+                def _():
+                    state_copy(o, k, 1).wait_recv()
+                    extra_ref[...] = states_ref[k, o, KEY_DIM:, :].astype(f32)
+                    total = extra_ref[8:9, :] + extra_ref[9:10, :] + extra_ref[10:11, :]
+                    state_ref[...] = state_ref[...] * jnp.exp(total) + states_ref[k, o, 0:KEY_DIM, :].astype(f32)
+
+                @pl.when(k == s - 1)
+                def _():
+                    product_ref[o, 8 - halo : 8, :] = extra_ref[0:halo, :] + extra_ref[halo : 2 * halo, :]
+
+        taps = [taps_ref[k : k + 1, lane(f, VALUE_DIM)] for k in range(CONV_TAPS)]
+        with scope("finish"):
+
+            @pl.loop(0, blocks)
+            def _(n):
+                at = pl.ds(pl.multiple_of(n * BLOCK_LEN, BLOCK_LEN), BLOCK_LEN)
+                state = before_ref[o, n] + jnp.exp(starts_ref[o, pl.ds(n, 1), :]) * state_ref[...]
+                output = intra_ref[o, at, :] + jnp.dot(
+                    decayed_ref[o, at, :], state.astype(bf16), preferred_element_type=f32
                 )
-            )
-        ]
-
-    def pass_state(o):
-        for d in range(1, n_sp):
-            for copy in state_copies(o, s, d):
-                start_when(s + d < n_sp, copy)
-
-    def finish(o, put):
-        state_ref[...] = jnp.zeros_like(state_ref)
-        product_ref[o, 0:8, :] = jnp.zeros((8, VALUE_DIM), f32)
-        for k in range(n_sp - 1):
-
-            @pl.when(k < s)
-            def _():
-                for copy in state_copies(o, k, 1):
-                    copy.wait_recv()
-                state_ref[...] = state_ref[...] * jnp.exp(extras_ref[k, o, halo : halo + 1, :]) + states_ref[
-                    k, o
-                ].astype(f32)
-
-            @pl.when(k == s - 1)
-            def _():
-                product_ref[o, 8 - halo : 8, :] = extras_ref[k, o, 0:halo, :]
-
-        taps = [taps_ref[k : k + 1, lane(f, VALUE_DIM)] for k in range(CONV_TAPS)]
-
-        @pl.loop(0, blocks)
-        def _(n):
-            at = pl.ds(pl.multiple_of(n * BLOCK_LEN, BLOCK_LEN), BLOCK_LEN)
-            state = before_ref[o, n] + jnp.exp(starts_ref[o, pl.ds(n, 1), :]) * state_ref[...]
-            output = intra_ref[o, at, :] + jnp.dot(
-                decayed_ref[o, at, :], state.astype(bf16), preferred_element_type=f32
-            )
-            output = output * lax.rsqrt(jnp.mean(output * output, axis=-1, keepdims=True) + EPSILON)
-            gate = part(o, at, 1).astype(f32)
-            ret_out = (output * (gate / (1.0 + jnp.exp(-gate)))).astype(bf16)
-            padded = product_ref[o, pl.ds(pl.multiple_of(n * BLOCK_LEN, 8), BLOCK_LEN + 8), :]
-            convolved = sum(
-                taps[k] * padded[8 - halo + k : 8 - halo + k + BLOCK_LEN, :] for k in range(CONV_TAPS)
-            )
-            conv_out = (part(o, at, 2).astype(f32) * convolved).astype(bf16)
-            put(at, ret_out, conv_out)
-
-    def send_mixed(o, i):
+                output = output * lax.rsqrt(jnp.mean(output * output, axis=-1, keepdims=True) + EPSILON)
+                gate = part(o, at, 1).astype(f32)
+                ret_out = (output * (gate / (1.0 + jnp.exp(-gate)))).astype(bf16)
+                padded = product_ref[o, pl.ds(pl.multiple_of(n * BLOCK_LEN, 8), BLOCK_LEN + 8), :]
+                convolved = sum(
+                    taps[k] * padded[8 - halo + k : 8 - halo + k + BLOCK_LEN, :] for k in range(CONV_TAPS)
+                )
+                conv_out = (part(o, at, 2).astype(f32) * convolved).astype(bf16)
+                put(at, ret_out, conv_out)
+
+    def mixed_out(o, i):
         def put(at, ret_out, conv_out):
             mixed_ref[i, at, 0:VALUE_DIM] = ret_out
             mixed_ref[i, at, VALUE_DIM:pair] = conv_out
 
         finish(o, put)
-        start(
-            remote(mixed_ref.at[i], merged_ref.at[:, lane(f, pair)], mixed_sent.at[i], mixed_landed.at[f], {"fs": o})
-        )
+        remote(
+            mixed_ref.at[i], merged_ref.at[:, lane(f, pair)], sent["mixed"], once_landed.at[2], {"fs": o}
+        ).start()
 
     def keep(at, ret_out, conv_out):
         merged_ref[at, lane(2 * f, VALUE_DIM)] = ret_out
         merged_ref[at, lane(2 * f + 1, VALUE_DIM)] = conv_out
 
-    def local_stage(o):
-        side_arrived(o)
-        project(o)
-        retain(o)
-        pass_state(o)
-
-    local_stage(xn)
-    local_stage(yn)
-    send_mixed(xn, 0)
-    arrived(dn, 0)
-    arrived(dn, 1)
-    local_stage(dn)
-    send_mixed(yn, 1)
-    out_step(1)
-
-    def slim_arrived(b, g):
-        remote(
-            slim(b, g), slim(b, g), slim_relay_sent.at[0], slim_landed.at[b, g], {"fs": g}
-        ).wait_recv()
-
-    def slim_relay(b, first, onward):
-        slim_arrived(b, first)
-        start(
-            remote(slim(b, first), slim(b, first), slim_relay_sent.at[b], slim_landed.at[b, first], {"fs": onward})
-        )
-
-    local_stage(f)
-    send_mixed(dn, 2)
-    for d in range(2, n_sp - 1):
-        out_step(d)
+    middle = range(2, n_sp - 1)
+    project_early(xn, 1)
+    project_early(yn, 2)
+    weight_step(n_sp - 1)
+    project_late(xn, 1)
+    retain(xn)
+    slim_step(1)
+    wide_line(s, xn)[0]()
+    project_late(yn, 2)
+    retain(yn)
+    for d in middle:
+        slim_step(d)
+    wide_step(1, f)
+    mixed_out(xn, 0)
+    mixed_out(yn, 1)
+    wide_step(1, xn)
+    with scope("x_third"):
+        arrived(dn, 0)
+        arrived(dn, 1)
+    for d in range(n_sp - 1):
+        slim_plane(d)
+    project(dn)
+    slim_step(n_sp - 1)
+    retain(dn)
+    wide_far()
+    wide_line(s, yn)[0]()
+    wide_line(s, dn)[0]()
+    project_late(f, 0)
+    for d in middle:
+        wide_step(d, f)
+    mixed_out(dn, 2)
+    slim_plane(n_sp - 1)
+    for d in middle:
+        wide_step(d, xn)
+    retain(f)
+    slim_relay(0)
+    wide_step(1, yn)
     finish(f, keep)
-    if n_sp > 2:
-        out_step(n_sp - 1)
-    for b in range(n_sp):
-        first, onward = (xn, yn) if b < n_sp // 2 else (yn, xn)
-        slim_relay(b, first, onward)
-    for p in order:
-        view = merged_ref.at[:, lane(p, pair)]
-        remote(view, view, mixed_sent.at[0], mixed_landed.at[p], {"fs": p}).wait_recv()
-    for b in range(n_sp):
-        slim_arrived(b, yn if b < n_sp // 2 else xn)
-        slim_arrived(b, dn)
-
-    tiles = part_ref.shape[0]
-    tile = part_ref.shape[2]
-
-    def partial_tile(core, i):
-        return lax.dot_general(
-            merged_ref[pl.ds(core * half, half), :],
-            outs_ref[pl.ds(pl.multiple_of(i * tile, tile), tile), :],
-            (((1,), (1,)), ((), ())),
-            preferred_element_type=f32,
-        ).astype(bf16)
-
-    def part_copy(i):
-        return remote(part_ref.at[i], far_ref.at[i], part_sent.at[i], part_landed.at[i], other)
-
-    @pl.loop(0, tiles)
-    def _(i):
-        part_ref[i] = partial_tile(1 - t, i)
-        part_copy(i).start()
-
-    @pl.loop(0, tiles)
-    def _(i):
-        mine = partial_tile(t, i).astype(f32)
-        part_copy(i).wait_recv()
-        out_ref[:, lane(i, tile)] = (mine + far_ref[i].astype(f32)).astype(bf16)
-
-    @pl.loop(0, tiles)
-    def _(i):
-        part_copy(i).wait_send()
-
-    for copy in waits:
-        copy.wait_send()
-    for condition, copy in guarded:
-
-        @pl.when(condition)
-        def _():
-            copy.wait_send()
+    wide_step(1, dn)
+    slim_relay(1)
+    for d in middle:
+        wide_step(d, yn)
+        wide_step(d, dn)
+    for d in range(2, n_sp):
+        slim_relay(d)
+    with scope("settle"):
+        all_sent("weight", pieces_ref.at[0 : len(order)])
+        all_sent("decay", decay_piece_ref.at[0 : len(order)])
+        all_sent("norm", normed_ref.at[0])
+        all_sent("relay", normed_ref.at[0, 0:half, :])
+        all_sent("side", normed_ref.at[0:2])
+        all_sent("wide", outs_ref.at[0 : 2 * cut, :])
+        all_sent("wide_relay", outs_ref.at[0:cut, :])
+        for way in ("up", "down"):
+            line_sent(way, lambda k: full_ref.at[0 : k * slab_rows, :])
+            line_sent("slim_" + way, lambda k: outs_ref.at[0 : k * (rows - cut), :])
+        for k in range(1, n_sp):
+
+            @pl.when(s == n_sp - 1 - k)
+            def _(k=k):
+                all_sent("state", states_ref.at[0:k])
+
+    with scope("h_wait"):
+        view = merged_ref.at[:, 0 : len(order) * pair]
+        remote(view, view, sent["mixed"], once_landed.at[2], other).wait_recv()
+
+    def part_copy(b):
+        return remote(part_ref.at[0, b], far_ref.at[b], sent["part"], part_landed.at[b], other)
+
+    def out_tile(b):
+        @pl.loop(0, 2)
+        def _(j):
+            core = jnp.where(j == 0, 1 - t, t)
+            part_ref[j, b] = lax.dot_general(
+                merged_ref[pl.ds(pl.multiple_of(core * half, half), half), :],
+                outs_ref[pl.ds(pl.multiple_of(b * slab_rows, slab_rows), slab_rows), :],
+                (((1,), (1,)), ((), ())),
+                preferred_element_type=f32,
+            ).astype(bf16)
+
+            @pl.when(j == 0)
+            def _():
+                part_copy(b).start()
+
+    def out_sum(k):
+        with scope("o_sum"):
+            b = nearest(k)
+            part_copy(b).wait_recv()
+            out_ref[:, lane(b, slab_rows)] = (part_ref[1, b].astype(f32) + far_ref[b].astype(f32)).astype(bf16)
+
+    for k in range(n_sp):
+        with scope(f"o_wait#k={k}"):
+            if k == n_sp - 1:
+                for g in (f,) + order:
+                    wide_step(k, g)
+            slim_rest(k)
+        with scope(f"o_tile#k={k}"):
+            out_tile(nearest(k))
+        if k > 0:
+            out_sum(k - 1)
+    with scope("o_settle"):
+        for way in ("up", "down"):
+            line_sent("wide_" + way, lambda k: outs_ref.at[0 : k * n_fs * cut, :])
+        all_sent("slim", outs_ref.at[0 : 2 * n_sp * (rows - cut), :])
+        all_sent("slim_relay", outs_ref.at[0 : n_sp * (rows - cut), :])
+        all_sent("mixed", mixed_ref)
+        all_sent("part", far_ref)
+    out_sum(n_sp - 1)
 
 
 def fast_shards(
@@ -812,7 +905,6 @@
     rows = query_weight.shape[0]
     width = 2 * KEY_DIM + 5 * VALUE_DIM
     lanes, pair = 2 * KEY_DIM, 2 * VALUE_DIM
-    tile = min(OUT_TILE, model)
 
     frequency = np.tile(1.0 / ROPE_BASE ** np.linspace(0.0, 1.0, KEY_DIM // 2), 4)
     near = np.arange(tok)[:, None] * frequency[None, :]
@@ -838,6 +930,7 @@
         ((n_fs, 8, BLOCK_LEN), f32),
         ((tok, lanes), f32),
         ((tok, lanes), f32),
+        ((n_fs - 1, tok, width), f32),
         ((n_fs, tok, width), bf16),
         ((n_fs, tok, VALUE_DIM), f32),
         ((n_fs, tok, KEY_DIM), bf16),
@@ -845,46 +938,25 @@
         ((n_fs, 8, VALUE_DIM), f32),
         ((n_fs, 8 + tok, VALUE_DIM), f32),
         ((KEY_DIM, VALUE_DIM), f32),
-        ((n_fs, KEY_DIM, VALUE_DIM), bf16),
-        ((n_sp, n_fs, KEY_DIM, VALUE_DIM), bf16),
-        ((n_fs, 8, VALUE_DIM), f32),
-        ((n_sp, n_fs, 8, VALUE_DIM), f32),
+        ((16, VALUE_DIM), f32),
+        ((n_fs, KEY_DIM + 16, VALUE_DIM), bf16),
+        ((n_sp, n_fs, KEY_DIM + 16, VALUE_DIM), bf16),
         ((n_fs - 1, tok, pair), bf16),
         ((tok, n_fs * pair), bf16),
-        ((model // tile, half, tile), bf16),
-        ((model // tile, half, tile), bf16),
+        ((2, n_sp, half, n_fs * rows), bf16),
+        ((n_sp, half, n_fs * rows), bf16),
     ]
     semaphores = [
-        (48,),
-        (3,),
-        (n_fs,),
-        (3,),
-        (n_fs,),
-        (4,),
-        (n_fs, 2),
-        (n_fs, 2),
-        (n_fs, 2),
-        (2,),
+        (8,),
+        (18,),
         (n_sp, n_fs),
         (n_sp, n_fs),
         (n_sp, n_fs),
-        (3,),
+        (n_fs, 2),
         (n_fs,),
         (n_sp, n_fs),
-        (n_sp, n_fs),
-        (n_sp, n_fs),
         (n_sp,),
-        (n_sp,),
-        (n_sp,),
-        (n_sp, 2),
-        (n_sp, n_fs),
-        (n_sp,),
-        (n_fs, n_sp, 2),
-        (n_sp, n_fs, 2),
-        (n_fs - 1,),
-        (n_fs,),
-        (model // tile,),
-        (model // tile,),
+        (3,),
     ]
     mixed = pl.pallas_call(
         lambda *refs: mixer_kernel(n_sp, *refs),
@@ -924,7 +996,7 @@
         tok, model = arrays[0].shape[1:]
         fits = n_fs == 4 and n_tp == 2 and n_sp > 2 and heads == n_fs
         fits = fits and conv_width == n_fs * VALUE_DIM and tok % (2 * BLOCK_LEN) == 0
-        fits = fits and tok // BLOCK_LEN <= 8 and model % OUT_TILE == 0
+        fits = fits and tok // BLOCK_LEN <= 8 and arrays[10].shape[0] % BLOCK_LEN == 0
         return (fast_shards if fits else shards)(*arrays)
 
     return chosen

time: 131 us -> 116 us (0.89)
  Pallas kernels: 127 us -> 113 us
    pallas_call x1, Pallas kernels: 127 us -> 113 us  [fast_shards(): pl.pallas_call(lambda *refs: mixer_kernel(n_sp, *refs), out_shape=jax.Sha...]
where the time goes in v2:
time: 116 us
  Pallas kernels  113 us (97%)
  local copies, waits for them, and re-layouts  2.73 us (2%)
    pallas_call x1, Pallas kernels, fast_shards(): pl.pallas_call(lambda *refs: mixer_kernel(n_sp, *refs), out_shape=jax.Sha...  113 us
    unnamed x1, local copies, waits for them, and re-layouts  2.73 us

profile of v2, /device:TPU:0, one launch (start us, length us, event | category | flops | bytes accessed | tf_op | source)
XLA Modules:
  0.0 115.7 jit_solution(1742463077907264731)
XLA Ops:
  0.0 113.0 %mixer.1 = bf16[384,2048]{1,0:T(8,128)(2,1)} custom-call(bf16[1,768,2048]{2,1,0:T(8,128)(2,1)} %refs_0_.1, f32[1,2048]{1,0:T(1,128)} %bitcast.3, bf16[128,256]{1,0:T(8,128)(2,1)} %refs_2_.1, bf16[128,256]{1,0:T(8,128)(2,1)} %refs_3_.1, bf16[128,512]{1,0:T(8,128)(2,1)} %refs_4_.1, bf16[128,512]{1,0:T(8,128)(2,1)} %refs_5_.1, bf16[128,512]{1,0:T(8,128)(2,1)} %refs_6_.1, ...), custom_call_target="tpu_custom_call" | custom-call | tf_op jit(solution)/shard_map/mixer/pallas_call | solution.py:961
  113.0 2.7 %copy.18 = bf16[1,384,2048]{2,1,0:T(8,128)(2,1)} copy(bf16[1,384,2048]{2,1,0:T(8,128)(2,1)} %bitcast.2) | data formatting | bytes 3145728

commit v3 on v2

--- a/solution.py
+++ b/solution.py
@@ -249,7 +249,7 @@
 def mixer_kernel(
     n_sp,
     tokens_ref,
-    gain_ref,
+    gain_source,
     query_ref,
     key_ref,
     value_ref,
@@ -257,14 +257,18 @@
     conv_b_ref,
     conv_c_ref,
     conv_in_ref,
-    taps_ref,
+    taps_source,
     out_ret_ref,
     out_conv_ref,
-    decay_ref,
+    decay_source,
     near_cos_ref,
     near_sin_ref,
+    base_source,
+    out_ref,
+    gain_ref,
+    taps_ref,
+    decay_ref,
     base_ref,
-    out_ref,
     raw_ref,
     normed_ref,
     pieces_ref,
@@ -364,6 +368,7 @@
 
     fetch(query_ref, heads_ref.at[0], 0)
     fetch(key_ref, heads_ref.at[1], 0)
+    fetch(decay_source, decay_ref, 8)
     wide_weights = (value_ref, gate_ref, conv_b_ref, conv_c_ref, conv_in_ref)
     for p in range(n_fs):
         for j, weight in enumerate(wide_weights):
@@ -391,6 +396,9 @@
                 outs_ref.at[own_rows(s, f), pl.ds(g * pair + j * VALUE_DIM, VALUE_DIM)],
                 5,
             )
+    fetch(gain_source, gain_ref, 9)
+    fetch(taps_source, taps_ref, 10)
+    fetch(base_source, base_ref, 11)
     tables = [fetch(near_cos_ref, cos_ref, 6), fetch(near_sin_ref, sin_ref, 7)]
 
     with scope("greet"):
@@ -403,6 +411,7 @@
         own = pl.ds(p * KEY_DIM, KEY_DIM)
         pieces_ref[p, :, 0:lanes] = jnp.concatenate([heads_ref[0, :, own], heads_ref[1, :, own]], axis=-1)
     full_ref[own_rows(s, f), 0:lanes] = pieces_ref[f, :, 0:lanes]
+    fetched(decay_ref, 8)
     decay_piece_ref[...] = jnp.zeros_like(decay_piece_ref)
     for p in range(n_fs):
         for n in range(blocks):
@@ -487,6 +496,7 @@
         remote(view, view, sent["side"], side_landed.at[owner], other).start()
 
     with scope("norm"):
+        fetched(gain_ref, 9)
         fetched(raw_ref.at[0:chunk, :], 3)
         normalise(0)
         norm_copy(f, 0, "norm", xn).start()
@@ -506,6 +516,8 @@
     for p in order[:2]:
         remote(wide(s, f), wide(s, f), sent["wide"], wide_landed.at[s, f], {"fs": p}).start()
 
+    fetched(taps_ref, 10)
+    fetched(base_ref, 11)
     for copy in tables:
         copy.wait()
 
@@ -774,17 +786,20 @@
         merged_ref[at, lane(2 * f + 1, VALUE_DIM)] = conv_out
 
     middle = range(2, n_sp - 1)
+    slim_plane(0)
     project_early(xn, 1)
     project_early(yn, 2)
     weight_step(n_sp - 1)
     project_late(xn, 1)
     retain(xn)
     slim_step(1)
+    slim_plane(1)
     wide_line(s, xn)[0]()
     project_late(yn, 2)
     retain(yn)
     for d in middle:
         slim_step(d)
+        slim_plane(d)
     wide_step(1, f)
     mixed_out(xn, 0)
     mixed_out(yn, 1)
@@ -792,9 +807,8 @@
     with scope("x_third"):
         arrived(dn, 0)
         arrived(dn, 1)
-    for d in range(n_sp - 1):
-        slim_plane(d)
     project(dn)
+    slim_relay(0)
     slim_step(n_sp - 1)
     retain(dn)
     wide_far()
@@ -803,21 +817,20 @@
     project_late(f, 0)
     for d in middle:
         wide_step(d, f)
+    slim_relay(1)
     mixed_out(dn, 2)
     slim_plane(n_sp - 1)
     for d in middle:
         wide_step(d, xn)
     retain(f)
-    slim_relay(0)
+    for d in middle:
+        slim_relay(d)
     wide_step(1, yn)
     finish(f, keep)
     wide_step(1, dn)
-    slim_relay(1)
     for d in middle:
         wide_step(d, yn)
         wide_step(d, dn)
-    for d in range(2, n_sp):
-        slim_relay(d)
     with scope("settle"):
         all_sent("weight", pieces_ref.at[0 : len(order)])
         all_sent("decay", decay_piece_ref.at[0 : len(order)])
@@ -864,6 +877,8 @@
             out_ref[:, lane(b, slab_rows)] = (part_ref[1, b].astype(f32) + far_ref[b].astype(f32)).astype(bf16)
 
     for k in range(n_sp):
+        if k == 1:
+            slim_relay(n_sp - 1)
         with scope(f"o_wait#k={k}"):
             if k == n_sp - 1:
                 for g in (f,) + order:
@@ -920,6 +935,10 @@
     dma = pltpu.SemaphoreType.DMA
     f32, bf16 = jnp.float32, jnp.bfloat16
     buffers = [
+        ((1, model), f32),
+        (conv_kernel.shape, f32),
+        (log_decay.shape, f32),
+        (base.shape, f32),
         ((half, model), bf16),
         ((n_fs, tok, model), bf16),
         ((n_fs, rows, width), bf16),
@@ -947,7 +966,7 @@
         ((n_sp, half, n_fs * rows), bf16),
     ]
     semaphores = [
-        (8,),
+        (12,),
         (18,),
         (n_sp, n_fs),
         (n_sp, n_fs),
@@ -958,17 +977,7 @@
         (n_sp,),
         (3,),
     ]
-    mixed = pl.pallas_call(
-        lambda *refs: mixer_kernel(n_sp, *refs),
-        out_shape=jax.ShapeDtypeStruct((half, model), bf16),
-        in_specs=[any_space, vmem] + [any_space] * 7 + [vmem] + [any_space] * 2 + [vmem] + [any_space] * 2 + [vmem],
-        out_specs=vmem,
-        scratch_shapes=[pltpu.VMEM(shape, kind) for shape, kind in buffers] + [dma(shape) for shape in semaphores],
-        compiler_params=pltpu.CompilerParams(
-            collective_id=0, has_side_effects=True, vmem_limit_bytes=60 * 1024 * 1024
-        ),
-        name="mixer",
-    )(
+    operands = (
         tokens,
         norm_gain.reshape(1, model),
         query_weight,
@@ -986,6 +995,17 @@
         jnp.asarray(np.sin(near), jnp.float32),
         jnp.asarray(base, jnp.float32),
     )
+    mixed = pl.pallas_call(
+        lambda *refs: mixer_kernel(n_sp, *refs),
+        out_shape=jax.ShapeDtypeStruct((half, model), bf16),
+        in_specs=[any_space] * len(operands),
+        out_specs=vmem,
+        scratch_shapes=[pltpu.VMEM(shape, kind) for shape, kind in buffers] + [dma(shape) for shape in semaphores],
+        compiler_params=pltpu.CompilerParams(
+            collective_id=0, has_side_effects=True, vmem_limit_bytes=50 * 1024 * 1024
+        ),
+        name="mixer",
+    )(*(pltpu.with_memory_space_constraint(x, pltpu.HBM) for x in operands))
     return mixed[None]
 
 

time: 116 us -> 113 us (0.974)
  local copies, waits for them, and re-layouts: 2.73 us -> 1.15 us
    unnamed x1, local copies, waits for them, and re-layouts: 2.73 us -> 1.15 us
where the time goes in v3:
time: 113 us
  Pallas kernels  112 us (99%)
  local copies, waits for them, and re-layouts  1.15 us (1%)
    pallas_call x1, Pallas kernels, fast_shards(): pl.pallas_call(lambda *refs: mixer_kernel(n_sp, *refs), out_shape=jax.Sha...  112 us

profile of v3, /device:TPU:0, one launch (start us, length us, event | category | flops | bytes accessed | tf_op | source)
XLA Modules:
  0.0 113.0 jit_solution(16918853472130631404)
XLA Ops:
  0.0 111.8 %mixer.1 = bf16[384,2048]{1,0:T(8,128)(2,1)S(1)} custom-call(bf16[1,768,2048]{2,1,0:T(8,128)(2,1)} %refs_0_.1, f32[1,2048]{1,0:T(1,128)} %bitcast.3, bf16[128,256]{1,0:T(8,128)(2,1)} %refs_2_.1, bf16[128,256]{1,0:T(8,128)(2,1)} %refs_3_.1, bf16[128,512]{1,0:T(8,128)(2,1)} %refs_4_.1, bf16[128,512]{1,0:T(8,128)(2,1)} %refs_5_.1, bf16[128,512]{1,0:T(8,128)(2,1)} %refs_6_.1, ...), custom_call_target="tpu_custom_call" | custom-call | tf_op jit(solution)/shard_map/mixer/pallas_call | solution.py:998
  111.8 1.1 %copy.18 = bf16[1,384,2048]{2,1,0:T(8,128)(2,1)} copy(bf16[1,384,2048]{2,1,0:T(8,128)(2,1)S(1)} %bitcast.2) | data formatting | bytes 3145728
